TPU v7x, 512 devices: a whole 4x4x16 slice. The times are simulated.
512 devices in a mesh: ep: 32 (over z, core), tp: 16 (over y, x).
Axes of the slice: x: 4, y: 4, z: 16, core: 2. Of those that a mesh axis runs over, the one named last changes fastest.
Arguments:
- mix_rows: bfloat16 [8192, 2048], P('ep', 'tp'), may hold values from -6 to 6
- mix_gain: bfloat16 [2048], replicated, may hold values from 0.099609375 to 1.8984375
- w_query: bfloat16 [2048, 2048], P(None, 'tp'), may hold values from -0.125 to 0.125
- w_forget: bfloat16 [2048, 2048], P(None, 'tp'), may hold values from -0.125 to 0.125
- w_input: bfloat16 [2048, 2048], P(None, 'tp'), may hold values from -0.125 to 0.125
- w_outgate: bfloat16 [2048, 2048], P(None, 'tp'), may hold values from -0.125 to 0.125
- forget_gap: float32 [2048], P('tp'), may hold values from 1e-05 to 0.1
- decay_extra: float32 [16, 8192], P('tp', 'ep'), may hold values from -0.7 to 0, as said below
- head_gain: bfloat16 [128], replicated, may hold values from 0.099609375 to 1.8984375
- w_mixout: bfloat16 [2048, 2048], P('tp'), may hold values from -0.125 to 0.125
- moe_rows: bfloat16 [8192, 2048], P('ep', 'tp'), may hold values from -6 to 6
- moe_gain: bfloat16 [2048], replicated, may hold values from 0.099609375 to 1.8984375
- route_ids: int32 [8192, 2], P('ep'), may hold values from 0 to 31, all different within a row; in each aligned block of 256 rows (0 to 255, 256 to 511, ...) at most 24 rows name the same one
- route_scores: float32 [8192, 2], P('ep'), may hold values from 0.05 to 1
- w_gate: bfloat16 [32, 2048, 3072], P('ep', None, 'tp'), may hold values from -0.125 to 0.125
- w_up: bfloat16 [32, 2048, 3072], P('ep', None, 'tp'), may hold values from -0.125 to 0.125
- w_down: bfloat16 [32, 3072, 2048], P('ep', 'tp'), may hold values from -0.109375 to 0.109375
Outputs:
- mix_out: bfloat16 [8192, 2048], P('ep', 'tp')
- moe_out: bfloat16 [8192, 2048], P('ep', 'tp')
Inputs may be any that keep to these rules, and one draw needn't show every extreme that they name: `route_ids`: each row names 2 different experts. Among the rows of one index of ep at most 24 name the same expert, a bound that at least one block reaches. `decay_extra`: never positive.
All inputs are finite; a program needn't handle non-finite values.
Results may differ from a plain program's by a relative error of at most 0.017.
Values may be sent and summed in bfloat16 or wider, within the bound.
A program may use at most 64 MiB of HBM per device.

v0:
```python
import jax
import jax.numpy as jnp
from jax import lax
from jax.sharding import Mesh
from jax.sharding import PartitionSpec as P

BLOCK = 64
EP = ("ep_0", "ep_1")
TP = ("tp_0", "tp_1")


epsilon = 1e-06
HIGHEST_PRECISION = lax.Precision.HIGHEST


def from_everyone(x, axis):
    count = lax.axis_size(axis)
    return lax.all_to_all(jnp.broadcast_to(x[None], (count, *x.shape)), axis, 0, 0, tiled=True)


def in_order(blocks, dim):
    shape = list(blocks.shape[1:])
    shape[dim] *= blocks.shape[0]
    return jnp.moveaxis(blocks, 0, dim).reshape(shape)


def gathered_copies(x, axis, dim):
    blocks = from_everyone(x, axis)
    return in_order(blocks, dim)


def by_axis(x, axes):
    for axis in axes:
        x = lax.psum(x, axis)
    return x


def filled_with(x, identity):
    return jax.tree.map(
        lambda part, zero: jnp.zeros_like(part) + jnp.asarray(zero, part.dtype), x, identity
    )


def all_in_one(x, axis):
    leaves = jax.tree.leaves(x)
    sequence = sorted(range(len(leaves)), key=lambda k: -leaves[k].size)
    width = (1, *leaves[sequence[0]].shape)[-1]
    lines = [
        jnp.pad(leaves[k].reshape(-1), (0, -leaves[k].size % width)).reshape(-1, width)
        for k in sequence
    ]
    both, at, found = (lax.all_gather(jnp.concatenate(lines), axis), 0, {})
    for k, line in zip(sequence, lines):
        share = both[:, at : at + len(line)].reshape(len(both), -1)
        found[k] = share[:, : leaves[k].size].reshape(-1, *leaves[k].shape)
        at += len(line)
    numbers = iter(range(len(leaves)))
    return jax.tree.map(lambda _: found[next(numbers)], x)


def entering(x, axes, combine, identity):
    before = start = filled_with(x, identity)
    subtotal = x
    for axis in reversed(axes):
        count, here = (lax.axis_size(axis), lax.axis_index(axis))
        pieces = all_in_one(
            jax.tree.map(
                lambda part, kind: part.astype(kind), subtotal, (jnp.bfloat16, jnp.bfloat16)
            ),
            axis,
        )
        inside, subtotal = (start, start)
        for k in range(count):
            passed = k < here
            subtotal = combine(
                subtotal, jax.tree.map(lambda part, own: part[k].astype(own.dtype), pieces, x)
            )
            inside = jax.tree.map(lambda new, old: jnp.where(passed, new, old), subtotal, inside)
        before = combine(inside, before)
    return before


def cut_along(x, dim, count):
    shape = x.shape
    blocks = x.reshape(*shape[:dim], count, shape[dim] // count, *shape[dim + 1 :])
    return jnp.moveaxis(blocks, dim, 0)


def sum_at_owner(x, axis, dim):
    count = lax.axis_size(axis)
    blocks = lax.all_to_all(cut_along(x, dim, count), axis, 0, 0, tiled=True)
    return jnp.sum(blocks.astype(jnp.float32), axis=0)


def rms_scale(rows, gain):
    values = rows.astype(jnp.float32)
    scale = lax.rsqrt(jnp.mean(values * values, axis=-1, keepdims=True) + epsilon)
    return values * scale * gain.astype(jnp.float32)


def block_recurrence(query_rows, key_in, value, log_forget, state):
    heads_count, length, key_dim = query_rows.shape
    block_list = length // BLOCK

    def split(values):
        return jnp.moveaxis(values.reshape(heads_count, block_list, BLOCK, values.shape[2]), 1, 0)

    causal = jnp.tril(jnp.ones((BLOCK, BLOCK), dtype=bool))[:, :, None]

    def advance(carry, inputs):
        query_block, key_block, value_block, forget_block = inputs
        running_state = jnp.cumsum(forget_block, axis=1)
        spread = running_state[:, :, None, :] - running_state[:, None, :, :]
        decay = jnp.exp(jnp.where(causal, spread, -jnp.inf))
        scores = jnp.einsum(
            "hid,hjd,hijd->hij", query_block, key_block, decay, precision=HIGHEST_PRECISION
        )
        output = jnp.einsum(
            "hid,hde->hie", query_block * jnp.exp(running_state), carry, precision=HIGHEST_PRECISION
        )
        output = output + jnp.einsum(
            "hij,hje->hie", scores, value_block, precision=HIGHEST_PRECISION
        )
        last = running_state[:, -1:, :]
        carry = carry * jnp.exp(last)[:, 0, :, None] + jnp.einsum(
            "hjd,hje->hde",
            key_block * jnp.exp(last - running_state),
            value_block,
            precision=HIGHEST_PRECISION,
        )
        return (carry, output)

    carry, outputs = lax.scan(
        advance, state, (split(query_rows), split(key_in), split(value), split(log_forget))
    )
    return (jnp.moveaxis(outputs, 0, 1).reshape(heads_count, length, value.shape[2]), carry)


def chain(earlier, later):
    return (earlier[0] * later[0], later[0][:, :, None] * earlier[1] + later[1])


def per_device(
    mix_rows,
    mix_gain,
    w_query,
    w_forget,
    w_input,
    w_outgate,
    forget_gap,
    decay_extra,
    head_gain,
    w_mixout,
    moe_rows,
    moe_gain,
    route_ids,
    route_scores,
    w_gate,
    w_up,
    w_down,
):
    col_width = mix_rows.shape[1]
    ep_count = lax.axis_size(EP)
    model_width = col_width * lax.axis_size(TP)
    mix_whole = gathered_copies(mix_rows, TP, 1)
    moe_values = moe_rows.astype(jnp.float32)
    squares = by_axis(jnp.sum(moe_values * moe_values, axis=1), TP)
    gain_cols = lax.dynamic_slice_in_dim(moe_gain, lax.axis_index(TP) * col_width, col_width, 0)
    expert_scale = lax.rsqrt(squares / model_width + epsilon)[:, None]
    moe_normed = (moe_values * expert_scale * gain_cols.astype(jnp.float32)).astype(jnp.bfloat16)
    mix_normed = rms_scale(mix_whole, mix_gain).astype(jnp.bfloat16)
    length = mix_normed.shape[0]
    heads_dev = decay_extra.shape[0]

    def heads(values):
        return values.reshape(length, heads_dev, -1).transpose(1, 0, 2)

    query_preactivation = jnp.dot(mix_normed, w_query, preferred_element_type=jnp.float32)
    forget_pre = jnp.dot(mix_normed, w_forget, preferred_element_type=jnp.float32)
    input_pre = jnp.dot(mix_normed, w_input, preferred_element_type=jnp.float32)
    outgate_pre = jnp.dot(mix_normed, w_outgate, preferred_element_type=jnp.float32)
    query_rows = heads(jax.nn.silu(query_preactivation))
    key_in = heads(forget_gap * jax.nn.sigmoid(-forget_pre))
    value = heads(input_pre)
    log_forget = jnp.log1p(-key_in) + decay_extra[:, :, None]
    start_state = jnp.zeros((heads_dev, query_rows.shape[2], value.shape[2]), jnp.float32)
    local_out, local_state = block_recurrence(query_rows, key_in, value, log_forget, start_state)
    running_state = jnp.cumsum(log_forget, axis=1)
    passing = jnp.exp(running_state[:, -1, :])
    carried_state = entering(
        (passing, local_state), EP, chain, (jnp.ones_like(passing), jnp.zeros_like(local_state))
    )[1]
    head_out = local_out + jnp.einsum(
        "won,wnd->wod",
        query_rows * jnp.exp(running_state),
        carried_state,
        precision=HIGHEST_PRECISION,
    )
    gated = rms_scale(head_out, head_gain) * heads(jax.nn.silu(outgate_pre))
    gated = gated.transpose(1, 0, 2).reshape(length, -1).astype(jnp.bfloat16)
    piece = w_mixout
    mix_sum = sum_at_owner(
        lax.dot_general(
            piece, gated, (((0,), (1,)), ((), ())), preferred_element_type=jnp.float32
        ).astype(jnp.bfloat16),
        TP,
        0,
    )
    mix_out = mix_sum.astype(jnp.bfloat16).T
    tok_count, top_count = route_ids.shape
    local_experts = w_gate.shape[0]
    expert_count = local_experts * ep_count
    capacity = tok_count * top_count * 3 // (2 * expert_count)
    weights = route_scores / jnp.sum(route_scores, axis=1, keepdims=True)
    chosen = route_ids.reshape(-1)
    onehot = (chosen[:, None] == jnp.arange(expert_count, dtype=jnp.int32)[None, :]).astype(
        jnp.int32
    )
    rank = jnp.sum((jnp.cumsum(onehot, axis=0) - 1) * onehot, axis=1)
    place = chosen * capacity + rank
    token = jnp.arange(tok_count * top_count, dtype=jnp.int32) // top_count
    table = jnp.full((expert_count * capacity,), tok_count, jnp.int32).at[place].set(token)
    padded = jnp.concatenate(
        [moe_normed, jnp.zeros((1, moe_normed.shape[1]), jnp.bfloat16)], axis=0
    )
    slots = padded[table].reshape(ep_count, local_experts, capacity, -1)
    arrived = lax.all_to_all(slots, EP, split_axis=0, concat_axis=0, tiled=True)
    piece = lax.all_gather(arrived, TP, axis=3, tiled=True)
    gate_acts = jnp.einsum("secd,edf->secf", piece, w_gate, preferred_element_type=jnp.float32)
    up_acts = jnp.einsum("secd,edf->secf", piece, w_up, preferred_element_type=jnp.float32)
    hidden = (jax.nn.silu(gate_acts) * up_acts).astype(jnp.bfloat16)
    piece = w_down
    product = jnp.einsum("secf,efo->osec", hidden, piece, preferred_element_type=jnp.float32)
    expert_sum = sum_at_owner(
        product.reshape(col_width * lax.axis_size(TP), -1).astype(jnp.bfloat16), TP, 0
    )
    outgoing = expert_sum.astype(jnp.bfloat16).reshape(col_width, ep_count, -1)
    returned = lax.all_to_all(outgoing, EP, split_axis=1, concat_axis=1, tiled=True)
    picked = jnp.take(returned.reshape(col_width, -1), place, axis=1).astype(jnp.float32)
    picked = picked.reshape(col_width, tok_count, top_count)
    moe_out = jnp.sum(picked * weights[None, :, :], axis=2).T.astype(jnp.bfloat16)
    return (mix_out, moe_out)


def solution(mesh):
    torus = Mesh(mesh.devices.reshape(16, 2, 4, 4), ("ep_0", "ep_1", "tp_0", "tp_1"))
    placed = (
        P(EP, TP),
        P(),
        P(None, TP),
        P(None, TP),
        P(None, TP),
        P(None, TP),
        P(TP),
        P(TP, EP),
        P(),
        P(TP, None),
        P(EP, TP),
        P(),
        P(EP, None),
        P(EP, None),
        P(EP, None, TP),
        P(EP, None, TP),
        P(EP, TP, None),
    )
    return jax.shard_map(
        per_device, mesh=torus, in_specs=placed, out_specs=(P(EP, TP), P(EP, TP)), check_vma=False
    )
```

profile of v0, /device:TPU:1, one launch (start us, length us, event | category | flops | bytes accessed | tf_op | source)
XLA Modules:
  0.0 261.4 jit_solution(10481239153342818669)
XLA Ops:
  10.0 9.5 %psum.14 = f32[256]{0:T(256)S(1)} all-reduce(f32[256]{0:T(256)S(1)} %fusion.59), channel_id=1, replica_groups=mesh['ep_0'=16,'ep_1'=2,'tp_0'=4,'tp_1'=4] {'tp_0'}, use_global_device_ids=true, to_apply=%region_12.13 | all-reduce | flops 256 | bytes 2048 | tf_op jit(solution)/shard_map/psum | solution.py:34
  19.6 8.5 %psum.15 = f32[256]{0:T(256)S(1)} all-reduce(f32[256]{0:T(256)S(1)} %psum.14), channel_id=1, replica_groups=mesh['ep_0'=16,'ep_1'=2,'tp_0'=4,'tp_1'=4] {'tp_1'}, use_global_device_ids=true, to_apply=%region_13.14 | all-reduce | flops 256 | bytes 2048 | tf_op jit(solution)/shard_map/psum | solution.py:34
  29.9 2.4 scatter_custom_fusion
  34.1 1.9 gather_fusion
  36.0 38.6 %all_to_all.25 = bf16[32,1,24,128]{3,2,1,0:T(8,128)(2,1)} all-to-all(bf16[32,1,24,128]{3,2,1,0:T(8,128)(2,1)S(1)} %bitcast.356), channel_id=1, replica_groups=mesh['ep_0'=16,'ep_1'=2,'tp_0'=4,'tp_1'=4] {'ep_0','ep_1'}, dimensions={0} | all-to-all | bytes 393216 | tf_op jit(solution)/shard_map/all_to_all | solution.py:227
  75.9 3.7 %all-to-all-start = ((bf16[16,256,128]{2,1,0:T(8,128)(2,1)}), bf16[16,256,128]{2,1,0:T(8,128)(2,1)S(1)}, u32[]{:S(2)}, u32[]{:S(2)}) async-start(bf16[16,256,128]{2,1,0:T(8,128)(2,1)} %broadcast_in_dim.40), calls=%async_computation | async-start | bytes 2097152 | tf_op jit(solution)/shard_map/all_to_all | solution.py:18
  80.3 14.8 %all-to-all-done = bf16[16,256,128]{2,1,0:T(8,128)(2,1)S(1)} async-done(((bf16[16,256,128]{2,1,0:T(8,128)(2,1)}), bf16[16,256,128]{2,1,0:T(8,128)(2,1)S(1)}, u32[]{:S(2)}, u32[]{:S(2)}) %all-to-all-start) | async-done | bytes 1048608 | tf_op jit(solution)/shard_map/all_to_all | solution.py:18
  95.9 1.6 convert_bitcast_fusion
  98.0 2.0 log-plus-one_add_fusion
  101.9 2.0 copy.99
  103.8 1.8 reshape.945
  106.3 1.5 convolution_bitcast_fusion.1
  107.8 15.4 %while.13 = (s32[]{:T(128)}, f32[1,128,128]{2,1,0:T(8,128)S(1)}, f32[4,1,64,128]{3,2,1,0:T(8,128)}, f32[4,1,64,128]{3,2,1,0:T(8,128)S(1)}, f32[4,1,64,128]{3,2,1...) while((s32[]{:T(128)}, f32[1,128,128]{2,1,0:T(8,128)S(1)}, ...), condition=%wide.region_3.0_spmd.clone, body=%wide.region_1.3_spmd.clone.sunk | while | flops 34693120 | bytes 5108352 | solution.py:133
  108.6 1.7 fusion.257
  112.5 1.7 fusion.257
  116.3 1.7 fusion.257
  120.2 1.7 fusion.257
  123.3 18.3 %all-gather.6.cloned.1.call-done = bf16[32,1,24,2048]{3,2,0,1:T(8,128)(2,1)} async-done(((bf16[32,1,24,128]{3,2,0,1:T(8,128)(2,1)}), bf16[32,1,24,2048]{3,2,0,1:T(8,128)(2,1)}) %all-gather.6.cloned.1.call-update) | async-done | bytes 3145744 | tf_op jit(solution)/shard_map/all_gather | solution.py:228
  141.6 3.0 %fusion.38 = f32[32,1,24,192]{3,2,0,1:T(8,128)S(1)} fusion(bf16[32,1,24,2048]{3,2,0,1:T(8,128)(2,1)} %all-gather.6.cloned.1.call-done, bf16[1,2048,192]{1,2,0:T(8,128)(2,1)S(1)} %copy-done.12), kind=kOutput, calls=%fused_computation.56 | convolution fusion | flops 603979776 | bytes 4521984 | tf_op jit(solution)/shard_map/secd,edf->secf/dot_general | solution.py:229
  146.8 2.5 copy.135
  149.3 4.8 %all-to-all-start.3 = ((bf16[16,128,768]{1,2,0:T(8,128)(2,1)}), bf16[16,128,768]{1,2,0:T(8,128)(2,1)}, u32[]{:S(2)}, u32[]{:S(2)}) async-start(bf16[16,128,768]{1,2,0:T(8,128)(2,1)} %bitcast.352), calls=%async_computation.3 | async-start | bytes 6291456 | tf_op jit(solution)/shard_map/all_to_all | solution.py:91
  154.2 3.9 %all-gather.2 = bf16[2,129,128]{2,1,0:T(8,128)(2,1)S(1)} all-gather(bf16[1,129,128]{2,1,0:T(8,128)(2,1)S(1)} %maximum_bitcast_fusion), channel_id=2, replica_groups=mesh['ep_0'=16,'ep_1'=2,'tp_0'=4,'tp_1'=4] {'ep_1'}, dimensions={0}, use_global_device_ids=true | all-gather | bytes 99072 | tf_op jit(solution)/shard_map/all_gather | solution.py:52
  158.2 29.2 %all-gather.3 = bf16[16,129,128]{2,1,0:T(8,128)(2,1)S(1)} all-gather(bf16[1,129,128]{2,1,0:T(8,128)(2,1)S(1)} %maximum_bitcast_fusion.1), channel_id=3, replica_groups=mesh['ep_0'=16,'ep_1'=2,'tp_0'=4,'tp_1'=4] {'ep_0'}, dimensions={0}, use_global_device_ids=true | all-gather | bytes 561408 | tf_op jit(solution)/shard_map/all_gather | solution.py:52
  187.4 1.4 multiply_reduce_fusion.2
  188.8 1.9 fusion.37
  192.0 4.9 %all-to-all-done.3 = bf16[16,128,768]{1,2,0:T(8,128)(2,1)} async-done(((bf16[16,128,768]{1,2,0:T(8,128)(2,1)}), bf16[16,128,768]{1,2,0:T(8,128)(2,1)}, u32[]{:S(2)}, u32[]{:S(2)}) %all-to-all-start.3) | async-done | bytes 3145760 | tf_op jit(solution)/shard_map/all_to_all | solution.py:91
  196.9 5.3 %all-to-all-start.1 = ((bf16[16,128,256]{1,2,0:T(8,128)(2,1)}), bf16[16,128,256]{1,2,0:T(8,128)(2,1)S(1)}, u32[]{:S(2)}, u32[]{:S(2)}) async-start(bf16[16,128,256]{1,2,0:T(8,128)(2,1)} %bitcast.318), calls=%async_computation.1 | async-start | bytes 2097152 | tf_op jit(solution)/shard_map/all_to_all | solution.py:91
  202.2 3.1 %reduce_sum.89 = bf16[128,768]{0,1:T(8,128)(2,1)} reduce(bf16[16,128,768]{1,2,0:T(8,128)(2,1)} %all-to-all-done.3, bf16[]{:T(256)} %constant.137.clone.1), dimensions={0}, to_apply=%region_15.16 | reduce | flops 1474560 | bytes 3342338 | tf_op jit(solution)/shard_map/reduce_sum | solution.py:92
  205.3 12.1 %all-to-all-done.1 = bf16[16,128,256]{1,2,0:T(8,128)(2,1)S(1)} async-done(((bf16[16,128,256]{1,2,0:T(8,128)(2,1)}), bf16[16,128,256]{1,2,0:T(8,128)(2,1)S(1)}, u32[]{:S(2)}, u32[]{:S(2)}) %all-to-all-start.1) | async-done | bytes 1048608 | tf_op jit(solution)/shard_map/all_to_all | solution.py:91
  217.4 15.0 %all-to-all-start.4 = ((bf16[128,32,24]{0,2,1:T(8,128)(2,1)}), bf16[128,32,24]{0,2,1:T(8,128)(2,1)S(1)}, u32[]{:S(2)}, u32[]{:S(2)}) async-start(bf16[128,32,24]{0,2,1:T(8,128)(2,1)} %bitcast.73), calls=%async_computation.4 | async-start | bytes 393216 | tf_op jit(solution)/shard_map/all_to_all | solution.py:238
  233.8 17.4 %all-to-all-done.4 = bf16[128,32,24]{0,2,1:T(8,128)(2,1)S(1)} async-done(((bf16[128,32,24]{0,2,1:T(8,128)(2,1)}), bf16[128,32,24]{0,2,1:T(8,128)(2,1)S(1)}, u32[]{:S(2)}, u32[]{:S(2)}) %all-to-all-start.4) | async-done | bytes 196640 | tf_op jit(solution)/shard_map/all_to_all | solution.py:238
  252.5 2.1 multiply_reduce_fusion.1
  (140 shorter events, 26.7 us)
Async XLA Ops:
  7.2 138.6 %copy-start = (bf16[1,192,2048]{2,1,0:T(8,128)(2,1)S(1)}, bf16[1,192,2048]{2,1,0:T(8,128)(2,1)}, u32[]{:S(2)}) copy-start(bf16[1,192,2048]{2,1,0:T(8,128)(2,1)} %param.35) | copy-start | bytes 2359300
  7.2 67.5 %copy-start.7 = (bf16[256,128]{1,0:T(8,128)(2,1)S(1)}, bf16[256,128]{1,0:T(8,128)(2,1)}, u32[]{:S(2)}) copy-start(bf16[256,128]{1,0:T(8,128)(2,1)} %param.19) | copy-start | bytes 196612
  36.0 43.8 %copy-start.10 = (bf16[2048]{0:T(1024)(128)(2,1)S(1)}, bf16[2048]{0:T(1024)(128)(2,1)}, u32[]{:S(2)}) copy-start(bf16[2048]{0:T(1024)(128)(2,1)} %param.20) | copy-start | bytes 12292
  36.0 43.8 %copy-start.17 = (bf16[128]{0:T(256)(128)(2,1)S(1)}, bf16[128]{0:T(256)(128)(2,1)}, u32[]{:S(2)}) copy-start(bf16[128]{0:T(256)(128)(2,1)} %param.27) | copy-start | bytes 772
  75.9 19.2 %all-to-all-start = ((bf16[16,256,128]{2,1,0:T(8,128)(2,1)}), bf16[16,256,128]{2,1,0:T(8,128)(2,1)S(1)}, u32[]{:S(2)}, u32[]{:S(2)}) async-start(bf16[16,256,128]{2,1,0:T(8,128)(2,1)} %broadcast_in_dim.40), calls=%async_computation | async-start | bytes 2097152 | tf_op jit(solution)/shard_map/all_to_all | solution.py:18
  79.5 62.1 %all-gather.6.cloned.1.call-start = ((), (), s32[]{:S(2)}) async-start(), calls=%async_computation.5 | async-start | bytes 3342336 | tf_op jit(solution)/shard_map/all_gather | solution.py:228
  95.9 2.1 copy-start.16
  95.9 2.1 copy-start.18
  97.6 3.2 %copy-start.14 = (bf16[2048,128]{1,0:T(8,128)(2,1)S(1)}, bf16[2048,128]{1,0:T(8,128)(2,1)}, u32[]{:S(2)}) copy-start(bf16[2048,128]{1,0:T(8,128)(2,1)} %param.21) | copy-start | bytes 1572868
  97.9 2.8 %copy-start.2 = (bf16[256,2048]{0,1:T(8,128)(2,1)}, bf16[256,2048]{0,1:T(8,128)(2,1)S(1)}, u32[]{:S(2)}) copy-start(bf16[256,2048]{0,1:T(8,128)(2,1)S(1)} %fusion.35) | copy-start | bytes 3145732
  97.9 3.9 %copy-start.1 = (f32[256,16,128]{0,2,1:T(8,128)S(1)}, f32[256,16,128]{0,2,1:T(8,128)}, u32[]{:S(2)}) copy-start(f32[256,16,128]{0,2,1:T(8,128)} %convert_bitcast_fusion) | copy-start | bytes 6291460
  103.8 1.8 copy-start.5
  107.8 33.8 %copy-start.12 = (bf16[1,2048,192]{1,2,0:T(8,128)(2,1)S(1)}, bf16[1,2048,192]{1,2,0:T(8,128)(2,1)}, u32[]{:S(2)}) copy-start(bf16[1,2048,192]{1,2,0:T(8,128)(2,1)} %param.33) | copy-start | bytes 2359300
  123.3 21.4 %copy-start.13 = (bf16[1,2048,192]{1,2,0:T(8,128)(2,1)S(1)}, bf16[1,2048,192]{1,2,0:T(8,128)(2,1)}, u32[]{:S(2)}) copy-start(bf16[1,2048,192]{1,2,0:T(8,128)(2,1)} %param.34) | copy-start | bytes 2359300
  141.6 3.1 %copy-start.11 = (bf16[32,1,24,2048]{3,2,0,1:T(8,128)(2,1)S(1)}, bf16[32,1,24,2048]{3,2,0,1:T(8,128)(2,1)}, u32[]{:S(2)}) copy-start(bf16[32,1,24,2048]{3,2,0,1:T(8,128)(2,1)} %all-gather.6.cloned.1.call-done) | copy-start | bytes 9437188
  149.3 4.9 %copy-start.6 = (f32[1,128,256]{1,2,0:T(8,128)S(1)}, f32[1,128,256]{1,2,0:T(8,128)}, u32[]{:S(2)}) copy-start(f32[1,128,256]{1,2,0:T(8,128)} %bitcast_add_fusion) | copy-start | bytes 393220
  149.3 38.1 %copy-start.15 = (f32[4,1,64,128]{3,2,1,0:T(8,128)S(1)}, f32[4,1,64,128]{3,2,1,0:T(8,128)}, u32[]{:S(2)}) copy-start(f32[4,1,64,128]{3,2,1,0:T(8,128)} %get-tuple-element.45) | copy-start | bytes 393220
  149.3 38.2 %copy-start.19 = (f32[256,128]{1,0:T(8,128)S(1)}, f32[256,128]{1,0:T(8,128)}, u32[]{:S(2)}) copy-start(f32[256,128]{1,0:T(8,128)} %get-tuple-element.153) | copy-start | bytes 393220
  149.3 47.6 %all-to-all-start.3 = ((bf16[16,128,768]{1,2,0:T(8,128)(2,1)}), bf16[16,128,768]{1,2,0:T(8,128)(2,1)}, u32[]{:S(2)}, u32[]{:S(2)}) async-start(bf16[16,128,768]{1,2,0:T(8,128)(2,1)} %bitcast.352), calls=%async_computation.3 | async-start | bytes 6291456 | tf_op jit(solution)/shard_map/all_to_all | solution.py:91
  154.1 34.7 %copy-start.3 = (bf16[256,2048]{0,1:T(8,128)(2,1)S(1)}, bf16[256,2048]{0,1:T(8,128)(2,1)}, u32[]{:S(2)}) copy-start(bf16[256,2048]{0,1:T(8,128)(2,1)} %copy-done.2) | copy-start | bytes 3145732
  154.1 34.7 %copy-start.4 = (bf16[128,2048]{1,0:T(8,128)(2,1)S(1)}, bf16[128,2048]{1,0:T(8,128)(2,1)}, u32[]{:S(2)}) copy-start(bf16[128,2048]{1,0:T(8,128)(2,1)} %param.28) | copy-start | bytes 1572868
  196.9 20.5 %all-to-all-start.1 = ((bf16[16,128,256]{1,2,0:T(8,128)(2,1)}), bf16[16,128,256]{1,2,0:T(8,128)(2,1)S(1)}, u32[]{:S(2)}, u32[]{:S(2)}) async-start(bf16[16,128,256]{1,2,0:T(8,128)(2,1)} %bitcast.318), calls=%async_computation.1 | async-start | bytes 2097152 | tf_op jit(solution)/shard_map/all_to_all | solution.py:91
  202.2 30.4 %copy-start.8 = (s32[256,2]{0,1:T(2,128)S(1)}, s32[256,2]{0,1:T(2,128)}, u32[]{:S(2)}) copy-start(s32[256,2]{0,1:T(2,128)} %param.31) | copy-start | bytes 6148
  202.2 30.6 %copy-start.9 = (f32[256,2]{0,1:T(2,128)S(1)}, f32[256,2]{0,1:T(2,128)}, u32[]{:S(2)}) copy-start(f32[256,2]{0,1:T(2,128)} %param.32) | copy-start | bytes 6148
  217.4 33.8 %all-to-all-start.4 = ((bf16[128,32,24]{0,2,1:T(8,128)(2,1)}), bf16[128,32,24]{0,2,1:T(8,128)(2,1)S(1)}, u32[]{:S(2)}, u32[]{:S(2)}) async-start(bf16[128,32,24]{0,2,1:T(8,128)(2,1)} %bitcast.73), calls=%async_computation.4 | async-start | bytes 393216 | tf_op jit(solution)/shard_map/all_to_all | solution.py:238
Sparse Core Ops, SparseCore 0:
  83.3 58.2 all-gather.5
where the time goes:
time: 262 us; the launch traced here: 261 us
  blocking collectives  89.7 us (34%)
  waiting for transfers between devices  67.9 us (26%)
  starting transfers between devices  29 us (11%)
  other arithmetic  23.6 us (9%)
  matrix products  18.3 us (7%)
  local copies, waits for them, and re-layouts  18.1 us (7%)
  between operations  14.6 us (6%)
    all_to_all x1, blocking collectives, per_device(): arrived = lax.all_to_all(slots, EP, split_axis=0, concat_axis=0, tiled=True)  38.6 us
    all_gather x2, blocking collectives, all_in_one(): both, at, found = (lax.all_gather(jnp.concatenate(lines), axis), 0, {})  33.1 us
    all_gather x1, waiting for transfers between devices, per_device(): piece = lax.all_gather(arrived, TP, axis=3, tiled=True)  18.3 us
    psum x2, blocking collectives, by_axis(): x = lax.psum(x, axis)  18 us
    all_to_all x1, waiting for transfers between devices, per_device(): lax.all_to_all(outgoing, EP, split_axis=1, concat_axis=1, tiled=True)  17.4 us
    all_to_all x2, waiting for transfers between devices, sum_at_owner(): blocks = lax.all_to_all(cut_along(x, dim, count), axis, 0, 0, tiled=True)  17 us
    all_to_all x1, starting transfers between devices, per_device(): lax.all_to_all(outgoing, EP, split_axis=1, concat_axis=1, tiled=True)  15 us
    all_to_all x1, waiting for transfers between devices, from_everyone(): lax.all_to_all(jnp.broadcast_to(x[None], (count, *x.shape)), axis, 0, 0,...  14.8 us
  transfers between devices with their start and end apart: 5, of which 5 were waited for; matrix products, arithmetic and copies ran while one was open for 14% of the time, Pallas kernels for 0%

commit v1 on v0

v1 whole, which is shorter than its diff:
```python
import functools

import jax
import jax.numpy as jnp
from jax import lax
from jax.experimental import pallas as pl
from jax.experimental.pallas import tpu as pltpu
from jax.sharding import PartitionSpec as P

MESH = pl.DeviceIdType.MESH
epsilon = 1e-06
HIGHEST = lax.Precision.HIGHEST
F32, BF16 = jnp.float32, jnp.bfloat16
SIDE = 4
COL = 128
GROUP = SIDE * COL


def dot(a, b):
    return jnp.dot(a, b, preferred_element_type=F32)


def dot_t(a, b):
    return lax.dot_general(a, b, (((1,), (1,)), ((), ())), preferred_element_type=F32)


def step_kernel(
    n_ep,
    cap,
    mix_rows,
    moe_rows,
    gains,
    gap,
    decay,
    head_gain,
    ids,
    scores,
    wq_h,
    wf_h,
    wi_h,
    wo_h,
    wmix_h,
    wg_h,
    wu_h,
    wd_h,
    mix_out,
    moe_out,
    wm,
    wmix,
    wg,
    wu,
    wd,
    slots,
    arrived,
    outgoing,
    returned,
    places,
    xa,
    xb,
    ma,
    mb,
    acc_x,
    sq_x,
    acc_g,
    acc_u,
    sq_m,
    st_out,
    st_in,
    st_back,
    st_enter,
    pxa,
    pxb,
    oxa,
    oxb,
    nxa,
    nxb,
    pma,
    pmb,
    oma,
    omb,
    nma,
    nmb,
    o2xa,
    o2xb,
    n2xa,
    n2xb,
    o2ma,
    o2mb,
    n2ma,
    n2mb,
    wsem,
    a2a_s,
    a2a_r,
    agx_s,
    agx_r,
    agm_s,
    agm_r,
    rsx_s,
    rsx_r,
    rsm_s,
    rsm_r,
):
    n_z = n_ep // 2
    ep = lax.axis_index("ep")
    tp = lax.axis_index("tp")
    x, y = lax.rem(tp, SIDE), tp // SIDE
    z, core = ep // 2, lax.rem(ep, 2)

    def on(v, d):
        return lax.rem(v + d + SIDE, SIDE)

    x_plus, x_minus = (ep, y * SIDE + on(x, 1)), (ep, y * SIDE + on(x, -1))
    y_plus, y_minus = (ep, on(y, 1) * SIDE + x), (ep, on(y, -1) * SIDE + x)

    loads = [
        pltpu.make_async_copy(src, dst, wsem.at[i])
        for i, (src, dst) in enumerate(
            [
                (wq_h, wm.at[:, 0:COL]),
                (wf_h, wm.at[:, COL : 2 * COL]),
                (wi_h, wm.at[:, 2 * COL : 3 * COL]),
                (wo_h, wm.at[:, 3 * COL : 4 * COL]),
                (wg_h.at[0], wg),
                (wu_h.at[0], wu),
                (wd_h.at[0], wd),
                (wmix_h, wmix),
            ]
        )
    ]
    for load in loads:
        load.start()

    barrier = pltpu.get_barrier_semaphore()
    for peer in (x_plus, x_minus, y_plus, y_minus):
        pl.semaphore_signal(barrier, inc=1, device_id=peer, device_id_type=MESH)

    def greet(o, carry):
        pl.semaphore_signal(
            barrier, inc=1, device_id=(lax.rem(ep + o, n_ep), tp), device_id_type=MESH
        )
        return carry

    lax.fori_loop(1, n_ep, greet, 0)

    tok = ids.shape[1]
    id0, id1 = ids[0:1], ids[1:2]
    expert = lax.broadcasted_iota(jnp.int32, (n_ep, tok), 0)
    one0, one1 = expert == id0, expert == id1
    named = jnp.where(one0 | one1, 1.0, 0.0).astype(BF16)
    row = lax.broadcasted_iota(jnp.int32, (tok, tok), 0)
    col = lax.broadcasted_iota(jnp.int32, (tok, tok), 1)
    before = jnp.where(row < col, 1.0, 0.0).astype(BF16)
    rank = dot(named, before)
    place0 = id0.astype(F32) * cap + jnp.sum(jnp.where(one0, rank, 0.0), axis=0, keepdims=True)
    place1 = id1.astype(F32) * cap + jnp.sum(jnp.where(one1, rank, 0.0), axis=0, keepdims=True)
    line = lax.broadcasted_iota(jnp.int32, (COL, tok), 0)
    table = jnp.where(line == 0, place0, place1)
    table = jnp.where(line == 2, scores[0:1], jnp.where(line == 3, scores[1:2], table))
    places[...] = table.T
    slot = lax.broadcasted_iota(jnp.int32, (n_ep * cap, tok), 0).astype(F32)
    pick = jnp.where((slot == place0) | (slot == place1), 1.0, 0.0).astype(BF16)
    slots[...] = dot(pick, moe_rows[...]).reshape(n_ep, cap, COL).astype(BF16)

    half_x = xa.shape[1]
    mine_a, mine_b = y * SIDE + x, x * SIDE + y
    xa[mine_a] = mix_rows[0:half_x]
    xb[mine_b] = mix_rows[half_x : 2 * half_x]

    pl.semaphore_wait(barrier, n_ep - 1 + 4)

    def exchange(src, dst, k):
        def send(o, carry):
            peer = lax.rem(ep + o, n_ep)
            pltpu.make_async_remote_copy(
                src_ref=src.at[peer],
                dst_ref=dst.at[ep],
                send_sem=a2a_s.at[k],
                recv_sem=a2a_r.at[k],
                device_id=(peer, tp),
                device_id_type=MESH,
            ).start()
            return carry

        lax.fori_loop(1, n_ep, send, 0)
        dst[ep] = src[ep]

    def whole(src, dst, k, count):
        return pltpu.make_async_remote_copy(
            src_ref=src.at[pl.ds(0, count)],
            dst_ref=dst.at[pl.ds(0, count)],
            send_sem=a2a_s.at[k],
            recv_sem=a2a_r.at[k],
            device_id=(lax.rem(ep + 1, n_ep), tp),
            device_id_type=MESH,
        )

    class Gather:
        def __init__(self, buf, outer, inner, out_plus, out_minus, in_plus, in_minus, s, r):
            self.buf, self.outer, self.inner = buf, outer, inner
            self.op, self.om, self.ip, self.im = out_plus, out_minus, in_plus, in_minus
            self.s, self.r = s, r
            self.h = buf.shape[1]

        def at(self, do, di):
            return on(self.outer, do) * SIDE + on(self.inner, di)

        def copy(self, block, rows, sem, to):
            ref = self.buf.at[block] if rows is None else self.buf.at[block, pl.ds(*rows)]
            return pltpu.make_async_remote_copy(
                src_ref=ref,
                dst_ref=ref,
                send_sem=self.s,
                recv_sem=self.r.at[sem],
                device_id=to,
                device_id_type=MESH,
            )

        def first(self):
            q = self.h // 2
            self.lo, self.hi = (0, q), (q, q)
            self.copy(self.at(0, 0), None, 0, self.ip).start()
            self.copy(self.at(0, 0), None, 1, self.im).start()

        def cross(self, di, sem):
            self.copy(self.at(0, di), None, sem, self.op).start()
            self.copy(self.at(0, di), None, sem + 1, self.om).start()

        def near(self):
            self.copy(self.at(0, -1), None, 0, self.ip).wait_recv()
            self.copy(self.at(0, -1), self.lo, 2, self.ip).start()
            self.copy(self.at(0, 1), None, 1, self.im).wait_recv()
            self.copy(self.at(0, 1), self.hi, 3, self.im).start()

        def far(self):
            self.copy(self.at(0, 2), self.lo, 2, self.ip).wait_recv()
            self.copy(self.at(0, 2), self.hi, 3, self.im).wait_recv()

        def relay(self, di, sem):
            self.copy(self.at(-1, di), None, sem, self.op).wait_recv()
            self.copy(self.at(-1, di), self.lo, sem + 2, self.op).start()
            self.copy(self.at(1, di), None, sem + 1, self.om).wait_recv()
            self.copy(self.at(1, di), self.hi, sem + 3, self.om).start()

        def last(self, di, sem):
            self.copy(self.at(2, di), self.lo, sem + 2, self.op).wait_recv()
            self.copy(self.at(2, di), self.hi, sem + 3, self.om).wait_recv()

        def drain(self):
            ref = self.buf.at[pl.ds(0, SIDE * SIDE - 1)]
            pltpu.make_async_remote_copy(
                src_ref=ref,
                dst_ref=ref,
                send_sem=self.s,
                recv_sem=self.r.at[0],
                device_id=self.op,
                device_id_type=MESH,
            ).wait_send()

    def gathers(a, b, s, r):
        return (
            Gather(a, y, x, y_plus, y_minus, x_plus, x_minus, s.at[0], r.at[0]),
            Gather(b, x, y, x_plus, x_minus, y_plus, y_minus, s.at[1], r.at[1]),
        )

    crossings = ((0, 4), (-1, 8), (1, 12), (2, 16))

    def gather_start(pair):
        for g in pair:
            g.first()
        for g in pair:
            g.cross(0, 4)

    def gather_near(pair):
        for g in pair:
            g.near()
        for g in pair:
            g.cross(-1, 8)
            g.cross(1, 12)

    def gather_far(pair):
        for g in pair:
            g.far()
            g.cross(2, 16)

    def gather_relays(pair):
        for di, sem in crossings:
            for g in pair:
                g.relay(di, sem)

    def gather_last(pair):
        for di, sem in crossings:
            for g in pair:
                g.last(di, sem)

    ones = jnp.ones((GROUP, COL), BF16)

    def features(is_a, group, j):
        return group * SIDE + j if is_a else j * SIDE + group

    def weight_rows(ref, is_a, group):
        if is_a:
            return ref[pl.ds(pl.multiple_of(group * GROUP, GROUP), GROUP), :]
        return jnp.concatenate(
            [
                ref[pl.ds(pl.multiple_of(features(False, group, j) * COL, COL), COL), :]
                for j in range(SIDE)
            ],
            axis=0,
        )

    def weight_columns(ref, is_a, group):
        if is_a:
            return ref[:, pl.ds(pl.multiple_of(group * GROUP, GROUP), GROUP)]
        return jnp.concatenate(
            [
                ref[:, pl.ds(pl.multiple_of(features(False, group, j) * COL, COL), COL)]
                for j in range(SIDE)
            ],
            axis=1,
        )

    def use_rows(buf, is_a, group, gain_at, outs, sq, start):
        h = buf.shape[1]
        scaled, squares = [], []
        for j in range(SIDE):
            part = buf[group * SIDE + j].astype(F32)
            scaled.append((part * gains[gain_at + features(is_a, group, j)]).astype(BF16))
            squares.append((part * part).astype(BF16))
        scaled, squares = jnp.concatenate(scaled, axis=1), jnp.concatenate(squares, axis=1)
        rows = pl.ds(0 if is_a else h, h)
        found = [(sq, dot(squares, ones))]
        for ref, acc in outs:
            if ref.shape[0] > ref.shape[1]:
                found.append((acc, dot(scaled, weight_rows(ref, is_a, group))))
            else:
                found.append((acc, dot_t(scaled, weight_columns(ref, is_a, group))))
        for acc, got in found:
            acc[rows, :] = got if start else acc[rows, :] + got

    class Scatter:
        def __init__(self, p, o1, n1, o2, n2, outer, inner, op, om, ip, im, s, r, make):
            self.p, self.o1, self.n1, self.o2, self.n2 = p, o1, n1, o2, n2
            self.outer, self.inner = outer, inner
            self.op, self.om, self.ip, self.im = op, om, ip, im
            self.s, self.r, self.make = s, r, make
            self.h = p.shape[1]
            self.q = self.h // 2
            self.lo, self.hi = pl.ds(0, self.q), pl.ds(self.q, self.q)

        def copy(self, src, dst, sem, to):
            return pltpu.make_async_remote_copy(
                src_ref=src,
                dst_ref=dst,
                send_sem=self.s,
                recv_sem=self.r.at[sem],
                device_id=to,
                device_id_type=MESH,
            )

        def produce(self, do):
            group = on(self.outer, do)
            got = self.make(group)
            for j in range(SIDE):
                self.p[group * SIDE + j] = got[:, j * COL : (j + 1) * COL].astype(BF16)

        def group(self, do, rows):
            return self.p.at[pl.ds(on(self.outer, do) * SIDE, SIDE), rows]

        def block(self, di, rows):
            return self.p.at[self.outer * SIDE + on(self.inner, di), rows]

        def leg1(self, name):
            return dict(
                a=lambda: self.copy(self.group(2, self.lo), self.o1.at[0], 0, self.op),
                b=lambda: self.copy(self.group(2, self.hi), self.o1.at[1], 1, self.om),
                c=lambda: self.copy(self.group(1, self.hi), self.n1.at[0, :, self.hi], 2, self.op),
                d=lambda: self.copy(self.group(-1, self.lo), self.n1.at[1, :, self.lo], 3, self.om),
                e=lambda: self.copy(self.group(1, self.lo), self.n1.at[0, :, self.lo], 4, self.op),
                f=lambda: self.copy(self.group(-1, self.hi), self.n1.at[1, :, self.hi], 5, self.om),
            )[name]()

        def leg2(self, name):
            return dict(
                a=lambda: self.copy(self.block(2, self.lo), self.o2.at[0], 6, self.ip),
                b=lambda: self.copy(self.block(2, self.hi), self.o2.at[1], 7, self.im),
                c=lambda: self.copy(self.block(1, self.hi), self.n2.at[0, self.hi], 8, self.ip),
                d=lambda: self.copy(self.block(-1, self.lo), self.n2.at[1, self.lo], 9, self.im),
                e=lambda: self.copy(self.block(1, self.lo), self.n2.at[0, self.lo], 10, self.ip),
                f=lambda: self.copy(self.block(-1, self.hi), self.n2.at[1, self.hi], 11, self.im),
            )[name]()

        def start1(self):
            self.produce(2)
            self.leg1("a").start()
            self.leg1("b").start()

        def direct1(self):
            self.produce(1)
            self.leg1("c").start()
            self.produce(-1)
            self.leg1("d").start()

        def add(self, dst, src):
            dst[...] = (dst[...].astype(F32) + src[...].astype(F32)).astype(BF16)

        def relay1(self):
            self.leg1("a").wait_recv()
            self.add(self.group(1, self.lo), self.o1.at[0])
            self.leg1("e").start()
            self.leg1("b").wait_recv()
            self.add(self.group(-1, self.hi), self.o1.at[1])
            self.leg1("f").start()

        def settle1(self):
            for leg in "cdef":
                self.leg1(leg).wait_recv()
            here = self.p.at[pl.ds(self.outer * SIDE, SIDE)]
            here[...] = (
                here[...].astype(F32) + self.n1[0].astype(F32) + self.n1[1].astype(F32)
            ).astype(BF16)
            for leg in "abcd":
                self.leg2(leg).start()

        def relay2(self):
            self.leg2("a").wait_recv()
            self.add(self.block(1, self.lo), self.o2.at[0])
            self.leg2("e").start()
            self.leg2("b").wait_recv()
            self.add(self.block(-1, self.hi), self.o2.at[1])
            self.leg2("f").start()

        def settle2(self):
            for leg in "cdef":
                self.leg2(leg).wait_recv()
            mine = self.p[self.outer * SIDE + self.inner].astype(F32)
            return mine + self.n2[0].astype(F32) + self.n2[1].astype(F32)

        def drain(self):
            ref = self.p.at[pl.ds(0, SIDE * SIDE - 1)]
            self.copy(ref, ref, 0, self.op).wait_send()

    def scatters(left, w, pa, pb, oa, ob, na, nb, o2a, o2b, n2a, n2b, s, r):
        h = pa.shape[1]

        def make_a(group):
            return dot(left()[0:h], weight_columns(w, True, group))

        def make_b(group):
            return dot(left()[h : 2 * h], weight_columns(w, False, group))

        return (
            Scatter(
                pa, oa, na, o2a, n2a, y, x, y_plus, y_minus, x_plus, x_minus, s.at[0], r.at[0], make_a
            ),
            Scatter(
                pb, ob, nb, o2b, n2b, x, y, x_plus, x_minus, y_plus, y_minus, s.at[1], r.at[1], make_b
            ),
        )

    def scatter_all(pair):
        for g in pair:
            g.start1()
        for g in pair:
            g.direct1()
        for g in pair:
            g.relay1()
        for g in pair:
            g.produce(0)
        for g in pair:
            g.settle1()
        for g in pair:
            g.relay2()
        got = [g.settle2() for g in pair]
        for g in pair:
            g.drain()
        return got

    exchange(slots, arrived, 0)
    mix = gathers(xa, xb, agx_s, agx_r)
    gather_start(mix)
    gather_near(mix)
    for load in loads[0:4]:
        load.wait()
    gather_far(mix)
    xo = [(wm, acc_x)]
    use_rows(xa, True, y, 0, xo, sq_x, True)
    use_rows(xb, False, x, 0, xo, sq_x, True)
    gather_relays(mix)
    for d in (-1, 1):
        use_rows(xa, True, on(y, d), 0, xo, sq_x, False)
        use_rows(xb, False, on(x, d), 0, xo, sq_x, False)
    gather_last(mix)
    use_rows(xa, True, on(y, 2), 0, xo, sq_x, False)
    use_rows(xb, False, on(x, 2), 0, xo, sq_x, False)
    for g in mix:
        g.drain()

    width = SIDE * SIDE * COL
    scale = lax.rsqrt(sq_x[...] * (1.0 / width) + epsilon)
    query = jax.nn.silu(acc_x[:, 0:COL] * scale)
    key = gap[...] * jax.nn.sigmoid(-(acc_x[:, COL : 2 * COL] * scale))
    value = (acc_x[:, 2 * COL : 3 * COL] * scale).astype(BF16)
    gate_out = jax.nn.silu(acc_x[:, 3 * COL : 4 * COL] * scale)
    extra = jnp.broadcast_to(decay[...], (COL, decay.shape[1])).T
    log_forget = jnp.log1p(-key) + extra
    part = half_x
    row = lax.broadcasted_iota(jnp.int32, (part, part), 0)
    col = lax.broadcasted_iota(jnp.int32, (part, part), 1)
    causal = row >= col
    lower = jnp.where(causal, 1.0, 0.0)
    outs, running, states, ends = [], [], [], []
    for c in range(2):
        rows = slice(c * part, (c + 1) * part)
        run = jnp.dot(lower, log_forget[rows], precision=HIGHEST, preferred_element_type=F32)
        mid, end = run[part // 2 - 1 : part // 2], run[part - 1 : part]
        q_in = (query[rows] * jnp.exp(run - mid)).astype(BF16)
        k_in = (key[rows] * jnp.exp(mid - run)).astype(BF16)
        near = lax.dot_general(q_in, k_in, (((1,), (1,)), ((), ())), preferred_element_type=F32)
        near = jnp.where(causal, near, 0.0).astype(BF16)
        outs.append(dot(near, value[rows]))
        k_end = (key[rows] * jnp.exp(end - run)).astype(BF16)
        states.append(
            lax.dot_general(value[rows], k_end, (((0,), (0,)), ((), ())), preferred_element_type=F32)
        )
        running.append(run)
        ends.append(end)
    q_second = (query[part:] * jnp.exp(running[1])).astype(BF16)
    outs[1] = outs[1] + lax.dot_general(
        q_second, states[0].astype(BF16), (((1,), (1,)), ((), ())), preferred_element_type=F32
    )
    state = states[0] * jnp.exp(ends[1]) + states[1]
    passing = jnp.exp(ends[0] + ends[1])
    q_enter = jnp.concatenate(
        [
            (query[:part] * jnp.exp(running[0])).astype(BF16),
            (query[part:] * jnp.exp(ends[0] + running[1])).astype(BF16),
        ],
        axis=0,
    )
    local_out = jnp.concatenate(outs, axis=0)
    slices = COL // 8
    st_out[...] = jnp.concatenate(
        [
            state.reshape(slices, 8, COL),
            jnp.broadcast_to(passing.reshape(1, 1, COL), (slices, 8, COL)),
        ],
        axis=1,
    ).astype(BF16)

    owner = core == lax.rem(z, 2)
    not_owner = jnp.logical_not(owner)

    def to_owner(k, carry):
        peer = 2 * k + lax.rem(k, 2)

        @pl.when(peer != ep)
        def _():
            pltpu.make_async_remote_copy(
                src_ref=st_out.at[k],
                dst_ref=st_in.at[ep],
                send_sem=a2a_s.at[2],
                recv_sem=a2a_r.at[2],
                device_id=(peer, tp),
                device_id_type=MESH,
            ).start()

        return carry

    lax.fori_loop(0, slices, to_owner, 0)

    @pl.when(owner)
    def _():
        st_in[ep] = st_out[z]

    whole(slots, arrived, 0, n_ep - 1).wait_recv()
    half_m = ma.shape[1]
    got = arrived[...].astype(F32).reshape(2 * half_m, COL).astype(BF16)
    ma[mine_a] = got[0:half_m]
    mb[mine_b] = got[half_m:]
    moe = gathers(ma, mb, agm_s, agm_r)
    gather_start(moe)
    for load in loads[4:]:
        load.wait()
    mo = [(wg, acc_g), (wu, acc_u)]
    moe_gain_at = SIDE * SIDE
    gather_near(moe)

    @pl.when(owner)
    def _():
        whole(st_in, st_in, 2, n_ep - 1).wait_recv()

        def chain(j, entering):
            block = st_in[j].astype(F32)
            st_back[j] = entering
            return block[8:16] * entering + block[0:8]

        lax.fori_loop(0, n_ep, chain, jnp.zeros((8, COL), F32))

        def give(o, carry):
            peer = lax.rem(ep + o, n_ep)
            pltpu.make_async_remote_copy(
                src_ref=st_back.at[peer],
                dst_ref=st_enter.at[z],
                send_sem=a2a_s.at[3],
                recv_sem=a2a_r.at[3],
                device_id=(peer, tp),
                device_id_type=MESH,
            ).start()
            return carry

        lax.fori_loop(1, n_ep, give, 0)
        st_enter[z] = st_back[ep]

    gather_far(moe)
    use_rows(ma, True, y, moe_gain_at, mo, sq_m, True)
    use_rows(mb, False, x, moe_gain_at, mo, sq_m, True)
    gather_relays(moe)
    for d in (-1, 1):
        use_rows(ma, True, on(y, d), moe_gain_at, mo, sq_m, False)
        use_rows(mb, False, on(x, d), moe_gain_at, mo, sq_m, False)
    gather_last(moe)
    use_rows(ma, True, on(y, 2), moe_gain_at, mo, sq_m, False)
    use_rows(mb, False, on(x, 2), moe_gain_at, mo, sq_m, False)
    for g in moe:
        g.drain()

    scale = lax.rsqrt(sq_m[:, 0:1] * (1.0 / width) + epsilon)
    hidden = (jax.nn.silu(acc_g[...] * scale) * (acc_u[...] * scale)).astype(BF16)
    pair = scatters(
        lambda: hidden, wd, pma, pmb, oma, omb, nma, nmb, o2ma, o2mb, n2ma, n2mb, rsm_s, rsm_r
    )
    got = scatter_all(pair)
    got = jnp.concatenate(got, axis=0)
    outgoing[...] = got.reshape(n_ep, cap, COL).astype(BF16)
    exchange(outgoing, returned, 1)

    @pl.when(owner)
    def _():
        whole(st_back, st_enter, 3, slices - 1).wait_recv()

    @pl.when(not_owner)
    def _():
        whole(st_back, st_enter, 3, slices).wait_recv()

    entering = st_enter[...].reshape(COL, COL).astype(BF16)
    head_out = local_out + lax.dot_general(
        q_enter, entering, (((1,), (1,)), ((), ())), preferred_element_type=F32
    )
    mean = jnp.mean(head_out * head_out, axis=1, keepdims=True)
    gated = head_out * lax.rsqrt(mean + epsilon) * head_gain[...].astype(F32) * gate_out
    gated = gated.astype(BF16)
    pair = scatters(
        lambda: gated, wmix, pxa, pxb, oxa, oxb, nxa, nxb, o2xa, o2xb, n2xa, n2xb, rsx_s, rsx_r
    )
    got = scatter_all(pair)
    mix_out[0:half_x] = got[0].astype(BF16)
    mix_out[half_x : 2 * half_x] = got[1].astype(BF16)

    score0, score1 = places[:, 2:3], places[:, 3:4]
    total = score0 + score1
    slot = lax.broadcasted_iota(jnp.int32, (tok, n_ep * cap), 1).astype(F32)
    weight = jnp.where(slot == places[:, 0:1], score0 / total, 0.0)
    weight = weight + jnp.where(slot == places[:, 1:2], score1 / total, 0.0)
    coarse = weight.astype(BF16)
    fine = (weight - coarse.astype(F32)).astype(BF16)
    whole(outgoing, returned, 1, n_ep - 1).wait_recv()
    results = returned[...].astype(F32).reshape(n_ep * cap, COL).astype(BF16)
    moe_out[...] = (dot(coarse, results) + dot(fine, results)).astype(BF16)

    whole(slots, arrived, 0, n_ep - 1).wait_send()
    whole(outgoing, returned, 1, n_ep - 1).wait_send()

    @pl.when(owner)
    def _():
        whole(st_out, st_in, 2, slices - 1).wait_send()
        whole(st_back, st_back, 3, n_ep - 1).wait_send()

    @pl.when(not_owner)
    def _():
        whole(st_out, st_in, 2, slices).wait_send()


def per_device(n_ep, *args):
    (
        mix_rows,
        mix_gain,
        w_query,
        w_forget,
        w_input,
        w_outgate,
        forget_gap,
        decay_extra,
        head_gain,
        w_mixout,
        moe_rows,
        moe_gain,
        route_ids,
        route_scores,
        w_gate,
        w_up,
        w_down,
    ) = args
    tok_a, tok_b = mix_rows.shape[0], moe_rows.shape[0]
    cap = tok_b * route_ids.shape[1] * 3 // (2 * n_ep)
    rows = n_ep * cap
    hidden = w_gate.shape[2]
    width = w_query.shape[0]
    gains = jnp.stack([mix_gain, moe_gain]).astype(F32).reshape(-1, 1, COL)
    hx, hm = tok_a // 2, rows // 2
    n_tp = SIDE * SIDE
    slices = COL // 8
    vmem = pl.BlockSpec(memory_space=pltpu.VMEM)
    hbm = pl.BlockSpec(memory_space=pltpu.HBM)
    dma = pltpu.SemaphoreType.DMA

    def v(shape, dtype=BF16):
        return pltpu.VMEM(shape, dtype)

    def scatter_buffers(h):
        return [
            v((n_tp, h, COL)),
            v((n_tp, h, COL)),
            v((2, SIDE, h // 2, COL)),
            v((2, SIDE, h // 2, COL)),
            v((2, SIDE, h, COL)),
            v((2, SIDE, h, COL)),
        ]

    def scatter_ends(h):
        return [v((2, h // 2, COL)), v((2, h // 2, COL)), v((2, h, COL)), v((2, h, COL))]

    scratch = [
        v((width, 4 * COL)),
        v((COL, width)),
        v((hidden, width)),
        v((hidden, width)),
        v((hidden, width)),
        v((n_ep, cap, COL)),
        v((n_ep, cap, COL)),
        v((n_ep, cap, COL)),
        v((n_ep, cap, COL)),
        v((tok_b, COL), F32),
        v((n_tp, hx, COL)),
        v((n_tp, hx, COL)),
        v((n_tp, hm, COL)),
        v((n_tp, hm, COL)),
        v((tok_a, 4 * COL), F32),
        v((tok_a, COL), F32),
        v((rows, hidden), F32),
        v((rows, hidden), F32),
        v((rows, COL), F32),
        v((slices, 16, COL)),
        v((n_ep, 16, COL)),
        v((n_ep, 8, COL), F32),
        v((slices, 8, COL), F32),
        *scatter_buffers(hx),
        *scatter_buffers(hm),
        *scatter_ends(hx),
        *scatter_ends(hm),
        dma((8,)),
        dma((4,)),
        dma((4,)),
        dma((2,)),
        dma((2, 20)),
        dma((2,)),
        dma((2, 20)),
        dma((2,)),
        dma((2, 12)),
        dma((2,)),
        dma((2, 12)),
    ]
    return pl.pallas_call(
        functools.partial(step_kernel, n_ep, cap),
        out_shape=[
            jax.ShapeDtypeStruct((tok_a, COL), BF16),
            jax.ShapeDtypeStruct((tok_b, COL), BF16),
        ],
        in_specs=[vmem] * 8 + [hbm] * 8,
        out_specs=[vmem, vmem],
        scratch_shapes=scratch,
        compiler_params=pltpu.CompilerParams(
            collective_id=0, has_side_effects=True, vmem_limit_bytes=60 * 1024 * 1024
        ),
    )(
        mix_rows,
        moe_rows,
        gains,
        forget_gap.reshape(1, COL),
        decay_extra,
        head_gain.reshape(1, COL),
        route_ids.T,
        route_scores.T,
        w_query,
        w_forget,
        w_input,
        w_outgate,
        w_mixout,
        jnp.swapaxes(w_gate, 1, 2),
        jnp.swapaxes(w_up, 1, 2),
        w_down,
    )


def solution(mesh):
    placed = (
        P("ep", "tp"),
        P(),
        P(None, "tp"),
        P(None, "tp"),
        P(None, "tp"),
        P(None, "tp"),
        P("tp"),
        P("tp", "ep"),
        P(),
        P("tp", None),
        P("ep", "tp"),
        P(),
        P("ep", None),
        P("ep", None),
        P("ep", None, "tp"),
        P("ep", None, "tp"),
        P("ep", "tp", None),
    )
    return jax.shard_map(
        functools.partial(per_device, mesh.shape["ep"]),
        mesh=mesh,
        in_specs=placed,
        out_specs=(P("ep", "tp"), P("ep", "tp")),
        check_vma=False,
    )
```

time: 262 us -> 98 us (0.37)
  the two profiles are of different devices: /device:TPU:1 before, /device:TPU:32 now
where the time goes in v1:
time: 98 us; the launch traced here: 97.7 us
  Pallas kernels  92.9 us (95%)
  local copies, waits for them, and re-layouts  4.14 us (4%)
    pallas_call x1, Pallas kernels, per_device(): pl.pallas_call(functools.partial(step_kernel, n_ep, cap), out_shape=[jax....  92.9 us
    unnamed x8, local copies, waits for them, and re-layouts  3.49 us

profile of v1, /device:TPU:32, one launch (start us, length us, event | category | flops | bytes accessed | tf_op | source)
XLA Modules:
  0.0 97.7 jit_solution(6242703798837522645)
XLA Ops:
  0.6 0.0 copy-start.1
  0.6 0.7 copy-done.1
  1.3 0.0 copy-start.2
  1.3 0.7 copy-done.2
  2.0 0.6 reshape.25.gains
  2.7 92.9 %shard_map.176 = (bf16[256,128]{1,0:T(8,128)(2,1)}, bf16[256,128]{1,0:T(8,128)(2,1)}) custom-call(bf16[256,128]{1,0:T(8,128)(2,1)} %mix_rows.1, bf16[256,128]{1,0:T(8,128)(2,1)} %moe_rows.1, f32[32,1,128]{2,1,0:T(1,128)} %reshape.25.gains, f32[1,128]{1,0:T(1,128)} %bitcast.10, f32[1,256]{1,0:T(1,128)} %decay.1, bf16[1,128]{1,0:T(2,128)(2,1)} %bitcast.11, ...), custom_call_target="tpu_custom_call" | custom-call | tf_op jit(solution)/shard_map/pallas_call | solution.py:772
  95.6 0.0 copy-start
  95.6 1.5 %copy.21 = bf16[256,128]{1,0:T(8,128)(2,1)} copy(bf16[256,128]{1,0:T(8,128)(2,1)} %get-tuple-element.4) | data formatting | bytes 131072
  97.1 0.0 copy-done
  97.1 0.6 copy.22
  (3 shorter events, 0.0 us)
Async XLA Ops:
  0.6 0.7 copy-start.1
  1.3 0.7 copy-start.2
  95.6 1.5 %copy-start = (bf16[256,128]{1,0:T(8,128)(2,1)S(1)}, bf16[256,128]{1,0:T(8,128)(2,1)}, u32[]{:S(2)}) copy-start(bf16[256,128]{1,0:T(8,128)(2,1)} %get-tuple-element.5) | copy-start | bytes 196612

commit v2 on v1

--- a/solution.py
+++ b/solution.py
@@ -29,7 +29,8 @@
     cap,
     mix_rows,
     moe_rows,
-    gains,
+    mix_gain,
+    moe_gain,
     gap,
     decay,
     head_gain,
@@ -55,6 +56,7 @@
     outgoing,
     returned,
     places,
+    gains,
     xa,
     xb,
     ma,
@@ -142,6 +144,9 @@
 
     lax.fori_loop(1, n_ep, greet, 0)
 
+    gains[0 : SIDE * SIDE] = mix_gain[...].astype(F32).reshape(SIDE * SIDE, 1, COL)
+    gains[SIDE * SIDE :] = moe_gain[...].astype(F32).reshape(SIDE * SIDE, 1, COL)
+
     tok = ids.shape[1]
     id0, id1 = ids[0:1], ids[1:2]
     expert = lax.broadcasted_iota(jnp.int32, (n_ep, tok), 0)
@@ -168,28 +173,56 @@
 
     pl.semaphore_wait(barrier, n_ep - 1 + 4)
 
-    def exchange(src, dst, k):
-        def send(o, carry):
-            peer = lax.rem(ep + o, n_ep)
-            pltpu.make_async_remote_copy(
-                src_ref=src.at[peer],
-                dst_ref=dst.at[ep],
-                send_sem=a2a_s.at[k],
-                recv_sem=a2a_r.at[k],
-                device_id=(peer, tp),
-                device_id_type=MESH,
-            ).start()
+    near_z = n_z // 4 - 1
+
+    def partner(u, c, away):
+        dz = u - near_z
+        return 2 * lax.rem(z + (dz if away else -dz) + 2 * n_z, n_z) + c
+
+    half_ep = n_ep // 2
+
+    def dispatch_copy(i):
+        u, c = i // 2, lax.rem(i, 2)
+        peer = partner(u, c, False)
+        return pltpu.make_async_remote_copy(
+            src_ref=slots.at[peer],
+            dst_ref=arrived.at[2 * u + core],
+            send_sem=a2a_s.at[0],
+            recv_sem=a2a_r.at[i // half_ep],
+            device_id=(peer, tp),
+            device_id_type=MESH,
+        )
+
+    def return_copy(i, chunk):
+        u, c = i // 2, lax.rem(i, 2)
+        peer = partner(u, c, True)
+        return pltpu.make_async_remote_copy(
+            src_ref=outgoing.at[i],
+            dst_ref=returned.at[ep],
+            send_sem=a2a_s.at[1],
+            recv_sem=a2a_r.at[2 + chunk],
+            device_id=(peer, tp),
+            device_id_type=MESH,
+        )
+
+    own_place = 2 * near_z + core
+
+    def send_all(make, first, count):
+        def send(i, carry):
+            @pl.when(i != own_place)
+            def _():
+                make(i).start()
+
             return carry
 
-        lax.fori_loop(1, n_ep, send, 0)
-        dst[ep] = src[ep]
-
-    def whole(src, dst, k, count):
+        lax.fori_loop(first, first + count, send, 0)
+
+    def whole(src, dst, k, count, r=None):
         return pltpu.make_async_remote_copy(
             src_ref=src.at[pl.ds(0, count)],
             dst_ref=dst.at[pl.ds(0, count)],
             send_sem=a2a_s.at[k],
-            recv_sem=a2a_r.at[k],
+            recv_sem=a2a_r.at[k if r is None else r],
             device_id=(lax.rem(ep + 1, n_ep), tp),
             device_id_type=MESH,
         )
@@ -276,16 +309,20 @@
         for g in pair:
             g.cross(-1, 8)
             g.cross(1, 12)
+        for g in pair:
+            g.relay(0, 4)
 
     def gather_far(pair):
         for g in pair:
             g.far()
             g.cross(2, 16)
+        for g in pair:
+            g.relay(-1, 8)
+            g.relay(1, 12)
 
     def gather_relays(pair):
-        for di, sem in crossings:
-            for g in pair:
-                g.relay(di, sem)
+        for g in pair:
+            g.relay(2, 16)
 
     def gather_last(pair):
         for di, sem in crossings:
@@ -319,7 +356,7 @@
             axis=1,
         )
 
-    def use_rows(buf, is_a, group, gain_at, outs, sq, start):
+    def use_rows(buf, is_a, group, gain_at, outs, sq, start, at=0):
         h = buf.shape[1]
         scaled, squares = [], []
         for j in range(SIDE):
@@ -327,7 +364,7 @@
             scaled.append((part * gains[gain_at + features(is_a, group, j)]).astype(BF16))
             squares.append((part * part).astype(BF16))
         scaled, squares = jnp.concatenate(scaled, axis=1), jnp.concatenate(squares, axis=1)
-        rows = pl.ds(0 if is_a else h, h)
+        rows = pl.ds(at if is_a else at + h, h)
         found = [(sq, dot(squares, ones))]
         for ref, acc in outs:
             if ref.shape[0] > ref.shape[1]:
@@ -457,215 +494,332 @@
             ),
         )
 
-    def scatter_all(pair):
+    def scatter_start(pair):
         for g in pair:
             g.start1()
         for g in pair:
             g.direct1()
+
+    def scatter_relay(pair):
         for g in pair:
             g.relay1()
         for g in pair:
             g.produce(0)
+
+    def scatter_settle(pair):
         for g in pair:
             g.settle1()
+
+    def scatter_relay2(pair):
         for g in pair:
             g.relay2()
+
+    def scatter_end(pair):
         got = [g.settle2() for g in pair]
         for g in pair:
             g.drain()
         return got
 
-    exchange(slots, arrived, 0)
+    live = {}
     mix = gathers(xa, xb, agx_s, agx_r)
-    gather_start(mix)
-    gather_near(mix)
-    for load in loads[0:4]:
-        load.wait()
-    gather_far(mix)
     xo = [(wm, acc_x)]
-    use_rows(xa, True, y, 0, xo, sq_x, True)
-    use_rows(xb, False, x, 0, xo, sq_x, True)
-    gather_relays(mix)
-    for d in (-1, 1):
-        use_rows(xa, True, on(y, d), 0, xo, sq_x, False)
-        use_rows(xb, False, on(x, d), 0, xo, sq_x, False)
-    gather_last(mix)
-    use_rows(xa, True, on(y, 2), 0, xo, sq_x, False)
-    use_rows(xb, False, on(x, 2), 0, xo, sq_x, False)
-    for g in mix:
-        g.drain()
+
+    def x_start():
+        gather_start(mix)
+
+    def x_near():
+        gather_near(mix)
+
+    def x_far():
+        gather_far(mix)
+        for load in loads[0:4]:
+            load.wait()
+        use_rows(xa, True, y, 0, xo, sq_x, True)
+        use_rows(xb, False, x, 0, xo, sq_x, True)
+
+    def x_relays():
+        gather_relays(mix)
+        for d in (-1, 1):
+            use_rows(xa, True, on(y, d), 0, xo, sq_x, False)
+            use_rows(xb, False, on(x, d), 0, xo, sq_x, False)
 
     width = SIDE * SIDE * COL
-    scale = lax.rsqrt(sq_x[...] * (1.0 / width) + epsilon)
-    query = jax.nn.silu(acc_x[:, 0:COL] * scale)
-    key = gap[...] * jax.nn.sigmoid(-(acc_x[:, COL : 2 * COL] * scale))
-    value = (acc_x[:, 2 * COL : 3 * COL] * scale).astype(BF16)
-    gate_out = jax.nn.silu(acc_x[:, 3 * COL : 4 * COL] * scale)
-    extra = jnp.broadcast_to(decay[...], (COL, decay.shape[1])).T
-    log_forget = jnp.log1p(-key) + extra
-    part = half_x
-    row = lax.broadcasted_iota(jnp.int32, (part, part), 0)
-    col = lax.broadcasted_iota(jnp.int32, (part, part), 1)
-    causal = row >= col
-    lower = jnp.where(causal, 1.0, 0.0)
-    outs, running, states, ends = [], [], [], []
-    for c in range(2):
-        rows = slice(c * part, (c + 1) * part)
-        run = jnp.dot(lower, log_forget[rows], precision=HIGHEST, preferred_element_type=F32)
-        mid, end = run[part // 2 - 1 : part // 2], run[part - 1 : part]
-        q_in = (query[rows] * jnp.exp(run - mid)).astype(BF16)
-        k_in = (key[rows] * jnp.exp(mid - run)).astype(BF16)
-        near = lax.dot_general(q_in, k_in, (((1,), (1,)), ((), ())), preferred_element_type=F32)
-        near = jnp.where(causal, near, 0.0).astype(BF16)
-        outs.append(dot(near, value[rows]))
-        k_end = (key[rows] * jnp.exp(end - run)).astype(BF16)
-        states.append(
-            lax.dot_general(value[rows], k_end, (((0,), (0,)), ((), ())), preferred_element_type=F32)
-        )
-        running.append(run)
-        ends.append(end)
-    q_second = (query[part:] * jnp.exp(running[1])).astype(BF16)
-    outs[1] = outs[1] + lax.dot_general(
-        q_second, states[0].astype(BF16), (((1,), (1,)), ((), ())), preferred_element_type=F32
-    )
-    state = states[0] * jnp.exp(ends[1]) + states[1]
-    passing = jnp.exp(ends[0] + ends[1])
-    q_enter = jnp.concatenate(
-        [
-            (query[:part] * jnp.exp(running[0])).astype(BF16),
-            (query[part:] * jnp.exp(ends[0] + running[1])).astype(BF16),
-        ],
-        axis=0,
-    )
-    local_out = jnp.concatenate(outs, axis=0)
+
+    def x_last():
+        gather_last(mix)
+        use_rows(xa, True, on(y, 2), 0, xo, sq_x, False)
+        use_rows(xb, False, on(x, 2), 0, xo, sq_x, False)
+        for g in mix:
+            g.drain()
+
+    def recurrence():
+        scale = lax.rsqrt(sq_x[...] * (1.0 / width) + epsilon)
+        query = jax.nn.silu(acc_x[:, 0:COL] * scale)
+        key = gap[...] * jax.nn.sigmoid(-(acc_x[:, COL : 2 * COL] * scale))
+        value = (acc_x[:, 2 * COL : 3 * COL] * scale).astype(BF16)
+        gate_out = jax.nn.silu(acc_x[:, 3 * COL : 4 * COL] * scale)
+        extra = jnp.broadcast_to(decay[...], (COL, decay.shape[1])).T
+        log_forget = jnp.log1p(-key) + extra
+        part = half_x
+        row = lax.broadcasted_iota(jnp.int32, (part, part), 0)
+        col = lax.broadcasted_iota(jnp.int32, (part, part), 1)
+        causal = row >= col
+        lower = jnp.where(causal, 1.0, 0.0)
+        outs, running, states, ends = [], [], [], []
+        for c in range(2):
+            rows = slice(c * part, (c + 1) * part)
+            run = jnp.dot(lower, log_forget[rows], precision=HIGHEST, preferred_element_type=F32)
+            mid, end = run[part // 2 - 1 : part // 2], run[part - 1 : part]
+            q_in = (query[rows] * jnp.exp(run - mid)).astype(BF16)
+            k_in = (key[rows] * jnp.exp(mid - run)).astype(BF16)
+            near = lax.dot_general(q_in, k_in, (((1,), (1,)), ((), ())), preferred_element_type=F32)
+            near = jnp.where(causal, near, 0.0).astype(BF16)
+            outs.append(dot(near, value[rows]))
+            k_end = (key[rows] * jnp.exp(end - run)).astype(BF16)
+            states.append(
+                lax.dot_general(value[rows], k_end, (((0,), (0,)), ((), ())), preferred_element_type=F32)
+            )
+            running.append(run)
+            ends.append(end)
+        q_second = (query[part:] * jnp.exp(running[1])).astype(BF16)
+        outs[1] = outs[1] + lax.dot_general(
+            q_second, states[0].astype(BF16), (((1,), (1,)), ((), ())), preferred_element_type=F32
+        )
+        state = states[0] * jnp.exp(ends[1]) + states[1]
+        passing = jnp.exp(ends[0] + ends[1])
+        q_enter = jnp.concatenate(
+            [
+                (query[:part] * jnp.exp(running[0])).astype(BF16),
+                (query[part:] * jnp.exp(ends[0] + running[1])).astype(BF16),
+            ],
+            axis=0,
+        )
+        local_out = jnp.concatenate(outs, axis=0)
+        st_out[...] = jnp.concatenate(
+            [
+                state.reshape(slices, 8, COL),
+                jnp.broadcast_to(passing.reshape(1, 1, COL), (slices, 8, COL)),
+            ],
+            axis=1,
+        ).astype(BF16)
+
+
+        def to_owner(k, carry):
+            peer = 2 * k + lax.rem(k, 2)
+
+            @pl.when(peer != ep)
+            def _():
+                pltpu.make_async_remote_copy(
+                    src_ref=st_out.at[k],
+                    dst_ref=st_in.at[ep],
+                    send_sem=a2a_s.at[2],
+                    recv_sem=a2a_r.at[4],
+                    device_id=(peer, tp),
+                    device_id_type=MESH,
+                ).start()
+
+            return carry
+
+        lax.fori_loop(0, slices, to_owner, 0)
+
+        @pl.when(owner)
+        def _():
+            st_in[ep] = st_out[z]
+        live.update(local_out=local_out, q_enter=q_enter, gate_out=gate_out)
+
     slices = COL // 8
-    st_out[...] = jnp.concatenate(
-        [
-            state.reshape(slices, 8, COL),
-            jnp.broadcast_to(passing.reshape(1, 1, COL), (slices, 8, COL)),
-        ],
-        axis=1,
-    ).astype(BF16)
-
     owner = core == lax.rem(z, 2)
     not_owner = jnp.logical_not(owner)
 
-    def to_owner(k, carry):
-        peer = 2 * k + lax.rem(k, 2)
-
-        @pl.when(peer != ep)
+    def chain_states():
+        @pl.when(owner)
         def _():
-            pltpu.make_async_remote_copy(
-                src_ref=st_out.at[k],
-                dst_ref=st_in.at[ep],
-                send_sem=a2a_s.at[2],
-                recv_sem=a2a_r.at[2],
-                device_id=(peer, tp),
-                device_id_type=MESH,
-            ).start()
-
-        return carry
-
-    lax.fori_loop(0, slices, to_owner, 0)
-
-    @pl.when(owner)
-    def _():
-        st_in[ep] = st_out[z]
-
-    whole(slots, arrived, 0, n_ep - 1).wait_recv()
-    half_m = ma.shape[1]
-    got = arrived[...].astype(F32).reshape(2 * half_m, COL).astype(BF16)
-    ma[mine_a] = got[0:half_m]
-    mb[mine_b] = got[half_m:]
-    moe = gathers(ma, mb, agm_s, agm_r)
-    gather_start(moe)
-    for load in loads[4:]:
-        load.wait()
-    mo = [(wg, acc_g), (wu, acc_u)]
+            whole(st_in, st_in, 2, n_ep - 1, 4).wait_recv()
+
+            def chain(j, entering):
+                block = st_in[j].astype(F32)
+                st_back[j] = entering
+                return block[8:16] * entering + block[0:8]
+
+            lax.fori_loop(0, n_ep, chain, jnp.zeros((8, COL), F32))
+
+            def give(o, carry):
+                peer = lax.rem(ep + o, n_ep)
+                pltpu.make_async_remote_copy(
+                    src_ref=st_back.at[peer],
+                    dst_ref=st_enter.at[z],
+                    send_sem=a2a_s.at[3],
+                    recv_sem=a2a_r.at[5],
+                    device_id=(peer, tp),
+                    device_id_type=MESH,
+                ).start()
+                return carry
+
+            lax.fori_loop(1, n_ep, give, 0)
+            st_enter[z] = st_back[ep]
+
     moe_gain_at = SIDE * SIDE
-    gather_near(moe)
-
-    @pl.when(owner)
-    def _():
-        whole(st_in, st_in, 2, n_ep - 1).wait_recv()
-
-        def chain(j, entering):
-            block = st_in[j].astype(F32)
-            st_back[j] = entering
-            return block[8:16] * entering + block[0:8]
-
-        lax.fori_loop(0, n_ep, chain, jnp.zeros((8, COL), F32))
-
-        def give(o, carry):
-            peer = lax.rem(ep + o, n_ep)
-            pltpu.make_async_remote_copy(
-                src_ref=st_back.at[peer],
-                dst_ref=st_enter.at[z],
-                send_sem=a2a_s.at[3],
-                recv_sem=a2a_r.at[3],
-                device_id=(peer, tp),
-                device_id_type=MESH,
-            ).start()
-            return carry
-
-        lax.fori_loop(1, n_ep, give, 0)
-        st_enter[z] = st_back[ep]
-
-    gather_far(moe)
-    use_rows(ma, True, y, moe_gain_at, mo, sq_m, True)
-    use_rows(mb, False, x, moe_gain_at, mo, sq_m, True)
-    gather_relays(moe)
-    for d in (-1, 1):
-        use_rows(ma, True, on(y, d), moe_gain_at, mo, sq_m, False)
-        use_rows(mb, False, on(x, d), moe_gain_at, mo, sq_m, False)
-    gather_last(moe)
-    use_rows(ma, True, on(y, 2), moe_gain_at, mo, sq_m, False)
-    use_rows(mb, False, on(x, 2), moe_gain_at, mo, sq_m, False)
-    for g in moe:
-        g.drain()
-
-    scale = lax.rsqrt(sq_m[:, 0:1] * (1.0 / width) + epsilon)
-    hidden = (jax.nn.silu(acc_g[...] * scale) * (acc_u[...] * scale)).astype(BF16)
-    pair = scatters(
-        lambda: hidden, wd, pma, pmb, oma, omb, nma, nmb, o2ma, o2mb, n2ma, n2mb, rsm_s, rsm_r
-    )
-    got = scatter_all(pair)
-    got = jnp.concatenate(got, axis=0)
-    outgoing[...] = got.reshape(n_ep, cap, COL).astype(BF16)
-    exchange(outgoing, returned, 1)
-
-    @pl.when(owner)
-    def _():
-        whole(st_back, st_enter, 3, slices - 1).wait_recv()
-
-    @pl.when(not_owner)
-    def _():
-        whole(st_back, st_enter, 3, slices).wait_recv()
-
-    entering = st_enter[...].reshape(COL, COL).astype(BF16)
-    head_out = local_out + lax.dot_general(
-        q_enter, entering, (((1,), (1,)), ((), ())), preferred_element_type=F32
-    )
-    mean = jnp.mean(head_out * head_out, axis=1, keepdims=True)
-    gated = head_out * lax.rsqrt(mean + epsilon) * head_gain[...].astype(F32) * gate_out
-    gated = gated.astype(BF16)
-    pair = scatters(
-        lambda: gated, wmix, pxa, pxb, oxa, oxb, nxa, nxb, o2xa, o2xb, n2xa, n2xb, rsx_s, rsx_r
-    )
-    got = scatter_all(pair)
-    mix_out[0:half_x] = got[0].astype(BF16)
-    mix_out[half_x : 2 * half_x] = got[1].astype(BF16)
-
-    score0, score1 = places[:, 2:3], places[:, 3:4]
-    total = score0 + score1
-    slot = lax.broadcasted_iota(jnp.int32, (tok, n_ep * cap), 1).astype(F32)
-    weight = jnp.where(slot == places[:, 0:1], score0 / total, 0.0)
-    weight = weight + jnp.where(slot == places[:, 1:2], score1 / total, 0.0)
-    coarse = weight.astype(BF16)
-    fine = (weight - coarse.astype(F32)).astype(BF16)
-    whole(outgoing, returned, 1, n_ep - 1).wait_recv()
-    results = returned[...].astype(F32).reshape(n_ep * cap, COL).astype(BF16)
-    moe_out[...] = (dot(coarse, results) + dot(fine, results)).astype(BF16)
+    half_m = ma.shape[2]
+    chunks = []
+
+    class Chunk:
+        def __init__(self, c):
+            self.c = c
+            self.a, self.b = ma.at[c], mb.at[c]
+            self.pair = gathers(self.a, self.b, agm_s.at[c], agm_r.at[c])
+            self.at = 2 * half_m * c
+            self.outs = [(wg, acc_g), (wu, acc_u)]
+
+        def use(self, d, start):
+            use_rows(self.a, True, on(y, d), moe_gain_at, self.outs, sq_m, start, self.at)
+            use_rows(self.b, False, on(x, d), moe_gain_at, self.outs, sq_m, start, self.at)
+
+        def start(self):
+            whole(slots, arrived, 0, half_ep - (1 if self.c == 0 else 0), self.c).wait_recv()
+            got = arrived[half_ep * self.c : half_ep * (self.c + 1)].astype(F32)
+            got = got.reshape(2 * half_m, COL).astype(BF16)
+            self.a[mine_a] = got[0:half_m]
+            self.b[mine_b] = got[half_m:]
+            gather_start(self.pair)
+
+        def near(self):
+            gather_near(self.pair)
+
+        def far(self):
+            gather_far(self.pair)
+            if self.c == 0:
+                for load in loads[4:6]:
+                    load.wait()
+            self.use(0, True)
+
+        def relays(self):
+            gather_relays(self.pair)
+            self.use(-1, False)
+            self.use(1, False)
+
+        def last(self):
+            gather_last(self.pair)
+            self.use(2, False)
+            for g in self.pair:
+                g.drain()
+
+        def experts(self):
+            if self.c == 0:
+                for load in loads[6:]:
+                    load.wait()
+            rows = pl.ds(self.at, 2 * half_m)
+            scale = lax.rsqrt(sq_m[rows, 0:1] * (1.0 / width) + epsilon)
+            hidden = (jax.nn.silu(acc_g[rows, :] * scale) * (acc_u[rows, :] * scale)).astype(BF16)
+            refs = [ref.at[self.c] for ref in (pma, pmb, oma, omb, nma, nmb, o2ma, o2mb, n2ma, n2mb)]
+            self.sums = scatters(lambda: hidden, wd, *refs, rsm_s.at[self.c], rsm_r.at[self.c])
+            scatter_start(self.sums)
+
+        def sum_relay(self):
+            scatter_relay(self.sums)
+
+        def sum_settle(self):
+            scatter_settle(self.sums)
+
+        def sum_relay2(self):
+            scatter_relay2(self.sums)
+
+        def give_back(self):
+            got = jnp.concatenate(scatter_end(self.sums), axis=0)
+            first = half_ep * self.c
+            outgoing[first : first + half_ep] = got.reshape(half_ep, cap, COL).astype(BF16)
+            send_all(lambda i: return_copy(i, self.c), first, half_ep)
+            if self.c == 0:
+                returned[ep] = outgoing[own_place]
+
+    near_chunk, far_chunk = Chunk(0), Chunk(1)
+
+    def x_sum_start():
+        @pl.when(owner)
+        def _():
+            whole(st_back, st_enter, 3, slices - 1, 5).wait_recv()
+
+        @pl.when(not_owner)
+        def _():
+            whole(st_back, st_enter, 3, slices, 5).wait_recv()
+
+        entering = st_enter[...].reshape(COL, COL).astype(BF16)
+        head_out = live["local_out"] + lax.dot_general(
+            live["q_enter"], entering, (((1,), (1,)), ((), ())), preferred_element_type=F32
+        )
+        mean = jnp.mean(head_out * head_out, axis=1, keepdims=True)
+        gated = head_out * lax.rsqrt(mean + epsilon) * head_gain[...].astype(F32) * live["gate_out"]
+        gated = gated.astype(BF16)
+        refs = (pxa, pxb, oxa, oxb, nxa, nxb, o2xa, o2xb, n2xa, n2xb)
+        live["sums"] = scatters(lambda: gated, wmix, *refs, rsx_s, rsx_r)
+        scatter_start(live["sums"])
+
+    def x_sum_relay():
+        scatter_relay(live["sums"])
+
+    def x_sum_settle():
+        scatter_settle(live["sums"])
+
+    def x_sum_relay2():
+        scatter_relay2(live["sums"])
+
+    def x_store():
+        got = scatter_end(live["sums"])
+        mix_out[0:half_x] = got[0].astype(BF16)
+        mix_out[half_x : 2 * half_x] = got[1].astype(BF16)
+
+    def weigh():
+        score0, score1 = places[:, 2:3], places[:, 3:4]
+        total = score0 + score1
+        slot = lax.broadcasted_iota(jnp.int32, (tok, n_ep * cap), 1).astype(F32)
+        weight = jnp.where(slot == places[:, 0:1], score0 / total, 0.0)
+        weight = weight + jnp.where(slot == places[:, 1:2], score1 / total, 0.0)
+        coarse = weight.astype(BF16)
+        fine = (weight - coarse.astype(F32)).astype(BF16)
+        live.update(coarse=coarse, fine=fine)
+
+    def combine():
+        whole(outgoing, returned, 1, half_ep - 1, 2).wait_recv()
+        whole(outgoing, returned, 1, half_ep, 3).wait_recv()
+        results = returned[...].astype(F32).reshape(n_ep * cap, COL).astype(BF16)
+        moe_out[...] = (dot(live["coarse"], results) + dot(live["fine"], results)).astype(BF16)
+
+    send_all(dispatch_copy, 0, half_ep)
+    x_start()
+    arrived[own_place] = slots[ep]
+    x_near()
+    send_all(dispatch_copy, half_ep, half_ep)
+    x_far()
+    near_chunk.start()
+    x_relays()
+    near_chunk.near()
+    x_last()
+    near_chunk.far()
+    far_chunk.start()
+    recurrence()
+    near_chunk.relays()
+    far_chunk.near()
+    near_chunk.last()
+    far_chunk.far()
+    near_chunk.experts()
+    chain_states()
+    far_chunk.relays()
+    far_chunk.last()
+    far_chunk.experts()
+    near_chunk.sum_relay()
+    far_chunk.sum_relay()
+    far_chunk.sum_settle()
+    near_chunk.sum_settle()
+    x_sum_start()
+    far_chunk.sum_relay2()
+    x_sum_relay()
+    far_chunk.give_back()
+    near_chunk.sum_relay2()
+    x_sum_settle()
+    near_chunk.give_back()
+    x_sum_relay2()
+    weigh()
+    x_store()
+    combine()
 
     whole(slots, arrived, 0, n_ep - 1).wait_send()
     whole(outgoing, returned, 1, n_ep - 1).wait_send()
@@ -705,8 +859,7 @@
     rows = n_ep * cap
     hidden = w_gate.shape[2]
     width = w_query.shape[0]
-    gains = jnp.stack([mix_gain, moe_gain]).astype(F32).reshape(-1, 1, COL)
-    hx, hm = tok_a // 2, rows // 2
+    hx, hm = tok_a // 2, rows // 4
     n_tp = SIDE * SIDE
     slices = COL // 8
     vmem = pl.BlockSpec(memory_space=pltpu.VMEM)
@@ -716,18 +869,18 @@
     def v(shape, dtype=BF16):
         return pltpu.VMEM(shape, dtype)
 
-    def scatter_buffers(h):
+    def scatter_buffers(h, n=()):
         return [
-            v((n_tp, h, COL)),
-            v((n_tp, h, COL)),
-            v((2, SIDE, h // 2, COL)),
-            v((2, SIDE, h // 2, COL)),
-            v((2, SIDE, h, COL)),
-            v((2, SIDE, h, COL)),
+            v((*n, n_tp, h, COL)),
+            v((*n, n_tp, h, COL)),
+            v((*n, 2, SIDE, h // 2, COL)),
+            v((*n, 2, SIDE, h // 2, COL)),
+            v((*n, 2, SIDE, h, COL)),
+            v((*n, 2, SIDE, h, COL)),
         ]
 
-    def scatter_ends(h):
-        return [v((2, h // 2, COL)), v((2, h // 2, COL)), v((2, h, COL)), v((2, h, COL))]
+    def scatter_ends(h, n=()):
+        return [v((*n, 2, h // 2, COL)), v((*n, 2, h // 2, COL)), v((*n, 2, h, COL)), v((*n, 2, h, COL))]
 
     scratch = [
         v((width, 4 * COL)),
@@ -740,10 +893,11 @@
         v((n_ep, cap, COL)),
         v((n_ep, cap, COL)),
         v((tok_b, COL), F32),
+        v((2 * n_tp, 1, COL), F32),
         v((n_tp, hx, COL)),
         v((n_tp, hx, COL)),
-        v((n_tp, hm, COL)),
-        v((n_tp, hm, COL)),
+        v((2, n_tp, hm, COL)),
+        v((2, n_tp, hm, COL)),
         v((tok_a, 4 * COL), F32),
         v((tok_a, COL), F32),
         v((rows, hidden), F32),
@@ -754,20 +908,20 @@
         v((n_ep, 8, COL), F32),
         v((slices, 8, COL), F32),
         *scatter_buffers(hx),
-        *scatter_buffers(hm),
+        *scatter_buffers(hm, (2,)),
         *scatter_ends(hx),
-        *scatter_ends(hm),
+        *scatter_ends(hm, (2,)),
         dma((8,)),
         dma((4,)),
-        dma((4,)),
+        dma((6,)),
         dma((2,)),
         dma((2, 20)),
-        dma((2,)),
-        dma((2, 20)),
+        dma((2, 2)),
+        dma((2, 2, 20)),
         dma((2,)),
         dma((2, 12)),
-        dma((2,)),
-        dma((2, 12)),
+        dma((2, 2)),
+        dma((2, 2, 12)),
     ]
     return pl.pallas_call(
         functools.partial(step_kernel, n_ep, cap),
@@ -775,7 +929,7 @@
             jax.ShapeDtypeStruct((tok_a, COL), BF16),
             jax.ShapeDtypeStruct((tok_b, COL), BF16),
         ],
-        in_specs=[vmem] * 8 + [hbm] * 8,
+        in_specs=[vmem] * 9 + [hbm] * 8,
         out_specs=[vmem, vmem],
         scratch_shapes=scratch,
         compiler_params=pltpu.CompilerParams(
@@ -784,7 +938,8 @@
     )(
         mix_rows,
         moe_rows,
-        gains,
+        mix_gain.reshape(-1, COL),
+        moe_gain.reshape(-1, COL),
         forget_gap.reshape(1, COL),
         decay_extra,
         head_gain.reshape(1, COL),

time: 98 us -> 85.8 us (0.88)
  the two profiles are of different devices: /device:TPU:32 before, /device:TPU:1 now
where the time goes in v2:
time: 85.8 us; the launch traced here: 85.5 us
  Pallas kernels  82.7 us (96%)
  local copies, waits for them, and re-layouts  2.14 us (2%)
    pallas_call x1, Pallas kernels, per_device(): pl.pallas_call(functools.partial(step_kernel, n_ep, cap), out_shape=[jax....  82.7 us
    unnamed x4, local copies, waits for them, and re-layouts  2.14 us

profile of v2, /device:TPU:1, one launch (start us, length us, event | category | flops | bytes accessed | tf_op | source)
XLA Modules:
  0.0 85.5 jit_solution(8162716702587043284)
XLA Ops:
  0.6 82.7 %shard_map.176 = (bf16[256,128]{1,0:T(8,128)(2,1)}, bf16[256,128]{1,0:T(8,128)(2,1)}) custom-call(bf16[256,128]{1,0:T(8,128)(2,1)} %mix_rows.1, bf16[256,128]{1,0:T(8,128)(2,1)} %moe_rows.1, bf16[16,128]{1,0:T(8,128)(2,1)} %bitcast.10, bf16[16,128]{1,0:T(8,128)(2,1)} %bitcast.11, f32[1,128]{1,0:T(1,128)} %bitcast.14, f32[1,256]{1,0:T(1,128)} %decay.1, ...), custom_call_target="tpu_custom_call" | custom-call | tf_op jit(solution)/shard_map/pallas_call | solution.py:926
  83.3 0.0 copy-start
  83.3 1.5 %copy.21 = bf16[256,128]{1,0:T(8,128)(2,1)} copy(bf16[256,128]{1,0:T(8,128)(2,1)} %get-tuple-element.4) | data formatting | bytes 131072
  84.8 0.0 copy-done
  84.8 0.6 copy.22
Async XLA Ops:
  83.3 1.5 %copy-start = (bf16[256,128]{1,0:T(8,128)(2,1)S(1)}, bf16[256,128]{1,0:T(8,128)(2,1)}, u32[]{:S(2)}) copy-start(bf16[256,128]{1,0:T(8,128)(2,1)} %get-tuple-element.5) | copy-start | bytes 196612

commit v3 on v2

--- a/solution.py
+++ b/solution.py
@@ -27,6 +27,25 @@
 def step_kernel(
     n_ep,
     cap,
+    mix_rows_h,
+    moe_rows_h,
+    mix_gain_h,
+    moe_gain_h,
+    gap_h,
+    decay_h,
+    head_gain_h,
+    ids_h,
+    scores_h,
+    wq_h,
+    wf_h,
+    wi_h,
+    wo_h,
+    wmix_h,
+    wg_h,
+    wu_h,
+    wd_h,
+    mix_out_h,
+    moe_out_h,
     mix_rows,
     moe_rows,
     mix_gain,
@@ -36,14 +55,6 @@
     head_gain,
     ids,
     scores,
-    wq_h,
-    wf_h,
-    wi_h,
-    wo_h,
-    wmix_h,
-    wg_h,
-    wu_h,
-    wd_h,
     mix_out,
     moe_out,
     wm,
@@ -90,6 +101,8 @@
     o2mb,
     n2ma,
     n2mb,
+    isem,
+    osem,
     wsem,
     a2a_s,
     a2a_r,
@@ -114,6 +127,36 @@
     x_plus, x_minus = (ep, y * SIDE + on(x, 1)), (ep, y * SIDE + on(x, -1))
     y_plus, y_minus = (ep, on(y, 1) * SIDE + x), (ep, on(y, -1) * SIDE + x)
 
+    barrier = pltpu.get_barrier_semaphore()
+    for peer in (x_plus, x_minus, y_plus, y_minus):
+        pl.semaphore_signal(barrier, inc=1, device_id=peer, device_id_type=MESH)
+
+    def greet(o, carry):
+        pl.semaphore_signal(
+            barrier, inc=1, device_id=(lax.rem(ep + o, n_ep), tp), device_id_type=MESH
+        )
+        return carry
+
+    lax.fori_loop(1, n_ep, greet, 0)
+
+    firsts = [
+        pltpu.make_async_copy(src, dst, isem.at[i])
+        for i, (src, dst) in enumerate(
+            [
+                (ids_h, ids),
+                (scores_h, scores),
+                (moe_rows_h, moe_rows),
+                (mix_rows_h, mix_rows),
+                (mix_gain_h, mix_gain),
+                (moe_gain_h, moe_gain),
+                (gap_h, gap),
+                (decay_h, decay),
+                (head_gain_h, head_gain),
+            ]
+        )
+    ]
+    for first in firsts:
+        first.start()
     loads = [
         pltpu.make_async_copy(src, dst, wsem.at[i])
         for i, (src, dst) in enumerate(
@@ -132,17 +175,8 @@
     for load in loads:
         load.start()
 
-    barrier = pltpu.get_barrier_semaphore()
-    for peer in (x_plus, x_minus, y_plus, y_minus):
-        pl.semaphore_signal(barrier, inc=1, device_id=peer, device_id_type=MESH)
-
-    def greet(o, carry):
-        pl.semaphore_signal(
-            barrier, inc=1, device_id=(lax.rem(ep + o, n_ep), tp), device_id_type=MESH
-        )
-        return carry
-
-    lax.fori_loop(1, n_ep, greet, 0)
+    for first in firsts:
+        first.wait()
 
     gains[0 : SIDE * SIDE] = mix_gain[...].astype(F32).reshape(SIDE * SIDE, 1, COL)
     gains[SIDE * SIDE :] = moe_gain[...].astype(F32).reshape(SIDE * SIDE, 1, COL)
@@ -374,6 +408,8 @@
         for acc, got in found:
             acc[rows, :] = got if start else acc[rows, :] + got
 
+    pieces = ((2,), (1, -1, 0))
+
     class Scatter:
         def __init__(self, p, o1, n1, o2, n2, outer, inner, op, om, ip, im, s, r, make):
             self.p, self.o1, self.n1, self.o2, self.n2 = p, o1, n1, o2, n2
@@ -400,70 +436,95 @@
             for j in range(SIDE):
                 self.p[group * SIDE + j] = got[:, j * COL : (j + 1) * COL].astype(BF16)
 
-        def group(self, do, rows):
-            return self.p.at[pl.ds(on(self.outer, do) * SIDE, SIDE), rows]
-
-        def block(self, di, rows):
-            return self.p.at[self.outer * SIDE + on(self.inner, di), rows]
-
-        def leg1(self, name):
-            return dict(
-                a=lambda: self.copy(self.group(2, self.lo), self.o1.at[0], 0, self.op),
-                b=lambda: self.copy(self.group(2, self.hi), self.o1.at[1], 1, self.om),
-                c=lambda: self.copy(self.group(1, self.hi), self.n1.at[0, :, self.hi], 2, self.op),
-                d=lambda: self.copy(self.group(-1, self.lo), self.n1.at[1, :, self.lo], 3, self.om),
-                e=lambda: self.copy(self.group(1, self.lo), self.n1.at[0, :, self.lo], 4, self.op),
-                f=lambda: self.copy(self.group(-1, self.hi), self.n1.at[1, :, self.hi], 5, self.om),
-            )[name]()
+        def row(self, do, di, rows):
+            return self.p.at[on(self.outer, do) * SIDE + on(self.inner, di), rows]
+
+        def outward(self, name, ds):
+            do, rows, buf, slot, sem, to = {
+                "a": (2, self.lo, self.o1, 0, 0, self.op),
+                "b": (2, self.hi, self.o1, 1, 1, self.om),
+                "c": (1, self.hi, self.n1, 0, 2, self.op),
+                "d": (-1, self.lo, self.n1, 1, 3, self.om),
+                "e": (1, self.lo, self.n1, 0, 4, self.op),
+                "f": (-1, self.hi, self.n1, 1, 5, self.om),
+            }[name]
+            sem = sem if len(ds) == 1 else sem + 6
+            whole_buf = buf is self.o1
+
+            def target(place):
+                return buf.at[slot, place] if whole_buf else buf.at[slot, place, rows]
+
+            three = pl.ds(0, len(ds))
+            pairs = [(self.row(do, di, rows), target(on(self.inner, di))) for di in ds]
+            pairs.append((self.p.at[three, rows], target(three)))
+            return [(src, dst, sem, to) for src, dst in pairs]
+
+        def send(self, name, ds):
+            for parts in self.outward(name, ds)[:-1]:
+                self.copy(*parts).start()
+
+        def wait(self, name, ds):
+            self.copy(*self.outward(name, ds)[-1]).wait_recv()
 
         def leg2(self, name):
-            return dict(
-                a=lambda: self.copy(self.block(2, self.lo), self.o2.at[0], 6, self.ip),
-                b=lambda: self.copy(self.block(2, self.hi), self.o2.at[1], 7, self.im),
-                c=lambda: self.copy(self.block(1, self.hi), self.n2.at[0, self.hi], 8, self.ip),
-                d=lambda: self.copy(self.block(-1, self.lo), self.n2.at[1, self.lo], 9, self.im),
-                e=lambda: self.copy(self.block(1, self.lo), self.n2.at[0, self.lo], 10, self.ip),
-                f=lambda: self.copy(self.block(-1, self.hi), self.n2.at[1, self.hi], 11, self.im),
-            )[name]()
+            di, rows, buf, slot, sem, to = {
+                "a": (2, self.lo, self.o2, 0, 12, self.ip),
+                "b": (2, self.hi, self.o2, 1, 13, self.im),
+                "c": (1, self.hi, self.n2, 0, 14, self.ip),
+                "d": (-1, self.lo, self.n2, 1, 15, self.im),
+                "e": (1, self.lo, self.n2, 0, 16, self.ip),
+                "f": (-1, self.hi, self.n2, 1, 17, self.im),
+            }[name]
+            dst = buf.at[slot] if buf is self.o2 else buf.at[slot, rows]
+            return self.copy(self.row(0, di, rows), dst, sem, to)
 
         def start1(self):
             self.produce(2)
-            self.leg1("a").start()
-            self.leg1("b").start()
+            for ds in pieces:
+                self.send("a", ds)
+                self.send("b", ds)
 
         def direct1(self):
             self.produce(1)
-            self.leg1("c").start()
+            for ds in pieces:
+                self.send("c", ds)
             self.produce(-1)
-            self.leg1("d").start()
+            for ds in pieces:
+                self.send("d", ds)
 
         def add(self, dst, src):
             dst[...] = (dst[...].astype(F32) + src[...].astype(F32)).astype(BF16)
 
-        def relay1(self):
-            self.leg1("a").wait_recv()
-            self.add(self.group(1, self.lo), self.o1.at[0])
-            self.leg1("e").start()
-            self.leg1("b").wait_recv()
-            self.add(self.group(-1, self.hi), self.o1.at[1])
-            self.leg1("f").start()
-
-        def settle1(self):
+        def relay1(self, ds):
+            self.wait("a", ds)
+            for di in ds:
+                self.add(self.row(1, di, self.lo), self.o1.at[0, on(self.inner, di)])
+            self.send("e", ds)
+            self.wait("b", ds)
+            for di in ds:
+                self.add(self.row(-1, di, self.hi), self.o1.at[1, on(self.inner, di)])
+            self.send("f", ds)
+
+        def settle1(self, ds):
             for leg in "cdef":
-                self.leg1(leg).wait_recv()
-            here = self.p.at[pl.ds(self.outer * SIDE, SIDE)]
-            here[...] = (
-                here[...].astype(F32) + self.n1[0].astype(F32) + self.n1[1].astype(F32)
-            ).astype(BF16)
-            for leg in "abcd":
-                self.leg2(leg).start()
+                self.wait(leg, ds)
+            for di in ds:
+                place = on(self.inner, di)
+                here = self.p.at[self.outer * SIDE + place]
+                here[...] = (
+                    here[...].astype(F32)
+                    + self.n1[0, place].astype(F32)
+                    + self.n1[1, place].astype(F32)
+                ).astype(BF16)
+                for leg in {2: "ab", 1: "c", -1: "d", 0: ""}[di]:
+                    self.leg2(leg).start()
 
         def relay2(self):
             self.leg2("a").wait_recv()
-            self.add(self.block(1, self.lo), self.o2.at[0])
+            self.add(self.row(0, 1, self.lo), self.o2.at[0])
             self.leg2("e").start()
             self.leg2("b").wait_recv()
-            self.add(self.block(-1, self.hi), self.o2.at[1])
+            self.add(self.row(0, -1, self.hi), self.o2.at[1])
             self.leg2("f").start()
 
         def settle2(self):
@@ -500,15 +561,17 @@
         for g in pair:
             g.direct1()
 
-    def scatter_relay(pair):
-        for g in pair:
-            g.relay1()
+    def scatter_relay(pair, piece):
+        for g in pair:
+            g.relay1(pieces[piece])
+
+    def scatter_own(pair):
         for g in pair:
             g.produce(0)
 
-    def scatter_settle(pair):
-        for g in pair:
-            g.settle1()
+    def scatter_settle(pair, piece):
+        for g in pair:
+            g.settle1(pieces[piece])
 
     def scatter_relay2(pair):
         for g in pair:
@@ -521,6 +584,10 @@
         return got
 
     live = {}
+    stores = [
+        pltpu.make_async_copy(mix_out, mix_out_h, osem.at[0]),
+        pltpu.make_async_copy(moe_out, moe_out_h, osem.at[1]),
+    ]
     mix = gathers(xa, xb, agx_s, agx_r)
     xo = [(wm, acc_x)]
 
@@ -532,7 +599,7 @@
 
     def x_far():
         gather_far(mix)
-        for load in loads[0:4]:
+        for load in loads:
             load.wait()
         use_rows(xa, True, y, 0, xo, sq_x, True)
         use_rows(xb, False, x, 0, xo, sq_x, True)
@@ -687,9 +754,6 @@
 
         def far(self):
             gather_far(self.pair)
-            if self.c == 0:
-                for load in loads[4:6]:
-                    load.wait()
             self.use(0, True)
 
         def relays(self):
@@ -704,21 +768,28 @@
                 g.drain()
 
         def experts(self):
-            if self.c == 0:
-                for load in loads[6:]:
-                    load.wait()
             rows = pl.ds(self.at, 2 * half_m)
             scale = lax.rsqrt(sq_m[rows, 0:1] * (1.0 / width) + epsilon)
             hidden = (jax.nn.silu(acc_g[rows, :] * scale) * (acc_u[rows, :] * scale)).astype(BF16)
             refs = [ref.at[self.c] for ref in (pma, pmb, oma, omb, nma, nmb, o2ma, o2mb, n2ma, n2mb)]
             self.sums = scatters(lambda: hidden, wd, *refs, rsm_s.at[self.c], rsm_r.at[self.c])
-            scatter_start(self.sums)
-
-        def sum_relay(self):
-            scatter_relay(self.sums)
-
-        def sum_settle(self):
-            scatter_settle(self.sums)
+
+        def sum_start(self):
+            for g in self.sums:
+                g.start1()
+
+        def sum_direct(self):
+            for g in self.sums:
+                g.direct1()
+
+        def sum_relay(self, piece):
+            scatter_relay(self.sums, piece)
+
+        def sum_own(self):
+            scatter_own(self.sums)
+
+        def sum_settle(self, piece):
+            scatter_settle(self.sums, piece)
 
         def sum_relay2(self):
             scatter_relay2(self.sums)
@@ -753,11 +824,14 @@
         live["sums"] = scatters(lambda: gated, wmix, *refs, rsx_s, rsx_r)
         scatter_start(live["sums"])
 
-    def x_sum_relay():
-        scatter_relay(live["sums"])
-
-    def x_sum_settle():
-        scatter_settle(live["sums"])
+    def x_sum_relay(piece):
+        scatter_relay(live["sums"], piece)
+
+    def x_sum_own():
+        scatter_own(live["sums"])
+
+    def x_sum_settle(piece):
+        scatter_settle(live["sums"], piece)
 
     def x_sum_relay2():
         scatter_relay2(live["sums"])
@@ -766,6 +840,7 @@
         got = scatter_end(live["sums"])
         mix_out[0:half_x] = got[0].astype(BF16)
         mix_out[half_x : 2 * half_x] = got[1].astype(BF16)
+        stores[0].start()
 
     def weigh():
         score0, score1 = places[:, 2:3], places[:, 3:4]
@@ -782,40 +857,54 @@
         whole(outgoing, returned, 1, half_ep, 3).wait_recv()
         results = returned[...].astype(F32).reshape(n_ep * cap, COL).astype(BF16)
         moe_out[...] = (dot(live["coarse"], results) + dot(live["fine"], results)).astype(BF16)
+        stores[1].start()
 
     send_all(dispatch_copy, 0, half_ep)
     x_start()
     arrived[own_place] = slots[ep]
     x_near()
     send_all(dispatch_copy, half_ep, half_ep)
+    near_chunk.start()
     x_far()
-    near_chunk.start()
+    near_chunk.near()
     x_relays()
-    near_chunk.near()
-    x_last()
     near_chunk.far()
     far_chunk.start()
-    recurrence()
+    x_last()
     near_chunk.relays()
     far_chunk.near()
+    recurrence()
     near_chunk.last()
     far_chunk.far()
     near_chunk.experts()
-    chain_states()
+    near_chunk.sum_start()
     far_chunk.relays()
+    near_chunk.sum_direct()
+    near_chunk.sum_own()
     far_chunk.last()
     far_chunk.experts()
-    near_chunk.sum_relay()
-    far_chunk.sum_relay()
-    far_chunk.sum_settle()
-    near_chunk.sum_settle()
+    far_chunk.sum_start()
+    far_chunk.sum_direct()
+    chain_states()
+    far_chunk.sum_relay(0)
+    far_chunk.sum_relay(1)
+    far_chunk.sum_own()
+    near_chunk.sum_relay(0)
+    near_chunk.sum_relay(1)
+    far_chunk.sum_settle(0)
+    far_chunk.sum_settle(1)
+    near_chunk.sum_settle(0)
+    far_chunk.sum_relay2()
+    near_chunk.sum_settle(1)
     x_sum_start()
-    far_chunk.sum_relay2()
-    x_sum_relay()
     far_chunk.give_back()
     near_chunk.sum_relay2()
-    x_sum_settle()
+    x_sum_relay(0)
+    x_sum_relay(1)
     near_chunk.give_back()
+    x_sum_own()
+    x_sum_settle(0)
+    x_sum_settle(1)
     x_sum_relay2()
     weigh()
     x_store()
@@ -832,6 +921,9 @@
     @pl.when(not_owner)
     def _():
         whole(st_out, st_in, 2, slices).wait_send()
+
+    for store in stores:
+        store.wait()
 
 
 def per_device(n_ep, *args):
@@ -862,7 +954,6 @@
     hx, hm = tok_a // 2, rows // 4
     n_tp = SIDE * SIDE
     slices = COL // 8
-    vmem = pl.BlockSpec(memory_space=pltpu.VMEM)
     hbm = pl.BlockSpec(memory_space=pltpu.HBM)
     dma = pltpu.SemaphoreType.DMA
 
@@ -883,6 +974,17 @@
         return [v((*n, 2, h // 2, COL)), v((*n, 2, h // 2, COL)), v((*n, 2, h, COL)), v((*n, 2, h, COL))]
 
     scratch = [
+        v((tok_a, COL)),
+        v((tok_b, COL)),
+        v((n_tp, COL)),
+        v((n_tp, COL)),
+        v((1, COL), F32),
+        v((1, tok_a), F32),
+        v((1, COL)),
+        v((2, tok_b), jnp.int32),
+        v((2, tok_b), F32),
+        v((tok_a, COL)),
+        v((tok_b, COL)),
         v((width, 4 * COL)),
         v((COL, width)),
         v((hidden, width)),
@@ -911,6 +1013,8 @@
         *scatter_buffers(hm, (2,)),
         *scatter_ends(hx),
         *scatter_ends(hm, (2,)),
+        dma((9,)),
+        dma((2,)),
         dma((8,)),
         dma((4,)),
         dma((6,)),
@@ -919,9 +1023,9 @@
         dma((2, 2)),
         dma((2, 2, 20)),
         dma((2,)),
-        dma((2, 12)),
+        dma((2, 18)),
         dma((2, 2)),
-        dma((2, 2, 12)),
+        dma((2, 2, 18)),
     ]
     return pl.pallas_call(
         functools.partial(step_kernel, n_ep, cap),
@@ -929,11 +1033,11 @@
             jax.ShapeDtypeStruct((tok_a, COL), BF16),
             jax.ShapeDtypeStruct((tok_b, COL), BF16),
         ],
-        in_specs=[vmem] * 9 + [hbm] * 8,
-        out_specs=[vmem, vmem],
+        in_specs=[hbm] * 17,
+        out_specs=[hbm, hbm],
         scratch_shapes=scratch,
         compiler_params=pltpu.CompilerParams(
-            collective_id=0, has_side_effects=True, vmem_limit_bytes=60 * 1024 * 1024
+            collective_id=0, has_side_effects=True, vmem_limit_bytes=63 * 1024 * 1024
         ),
     )(
         mix_rows,

time: 85.8 us -> 81.9 us (0.955)
  Pallas kernels: 82.7 us -> 78.9 us
    pallas_call x1, Pallas kernels: 82.7 us -> 78.9 us  [per_device(): pl.pallas_call(functools.partial(step_kernel, n_ep, cap), out_shape=[jax....]
where the time goes in v3:
time: 81.9 us; the launch traced here: 81.7 us
  Pallas kernels  78.9 us (96%)
  local copies, waits for them, and re-layouts  2.14 us (3%)
    pallas_call x1, Pallas kernels, per_device(): pl.pallas_call(functools.partial(step_kernel, n_ep, cap), out_shape=[jax....  78.9 us
    unnamed x4, local copies, waits for them, and re-layouts  2.14 us

profile of v3, /device:TPU:1, one launch (start us, length us, event | category | flops | bytes accessed | tf_op | source)
XLA Modules:
  0.0 81.7 jit_solution(9242097235566918265)
XLA Ops:
  0.6 78.9 %shard_map.176 = (bf16[256,128]{1,0:T(8,128)(2,1)}, bf16[256,128]{1,0:T(8,128)(2,1)}) custom-call(bf16[256,128]{1,0:T(8,128)(2,1)} %mix_rows_h.1, bf16[256,128]{1,0:T(8,128)(2,1)} %moe_rows_h.1, bf16[16,128]{1,0:T(8,128)(2,1)} %bitcast.10, bf16[16,128]{1,0:T(8,128)(2,1)} %bitcast.11, f32[1,128]{1,0:T(1,128)} %bitcast.14, f32[1,256]{1,0:T(1,128)} %decay_h.1, ...), custom_call_target="tpu_custom_call" | custom-call | tf_op jit(solution)/shard_map/pallas_call | solution.py:1030
  79.6 0.0 copy-start
  79.6 1.5 %copy.21 = bf16[256,128]{1,0:T(8,128)(2,1)} copy(bf16[256,128]{1,0:T(8,128)(2,1)} %get-tuple-element.4) | data formatting | bytes 131072
  81.1 0.0 copy-done
  81.1 0.6 copy.22
Async XLA Ops:
  79.6 1.5 %copy-start = (bf16[256,128]{1,0:T(8,128)(2,1)S(1)}, bf16[256,128]{1,0:T(8,128)(2,1)}, u32[]{:S(2)}) copy-start(bf16[256,128]{1,0:T(8,128)(2,1)} %get-tuple-element.5) | copy-start | bytes 196612

commit v4 on v3

--- a/solution.py
+++ b/solution.py
@@ -44,8 +44,8 @@
     wg_h,
     wu_h,
     wd_h,
-    mix_out_h,
-    moe_out_h,
+    mix_out,
+    moe_out,
     mix_rows,
     moe_rows,
     mix_gain,
@@ -55,8 +55,6 @@
     head_gain,
     ids,
     scores,
-    mix_out,
-    moe_out,
     wm,
     wmix,
     wg,
@@ -102,7 +100,6 @@
     n2ma,
     n2mb,
     isem,
-    osem,
     wsem,
     a2a_s,
     a2a_r,
@@ -127,18 +124,6 @@
     x_plus, x_minus = (ep, y * SIDE + on(x, 1)), (ep, y * SIDE + on(x, -1))
     y_plus, y_minus = (ep, on(y, 1) * SIDE + x), (ep, on(y, -1) * SIDE + x)
 
-    barrier = pltpu.get_barrier_semaphore()
-    for peer in (x_plus, x_minus, y_plus, y_minus):
-        pl.semaphore_signal(barrier, inc=1, device_id=peer, device_id_type=MESH)
-
-    def greet(o, carry):
-        pl.semaphore_signal(
-            barrier, inc=1, device_id=(lax.rem(ep + o, n_ep), tp), device_id_type=MESH
-        )
-        return carry
-
-    lax.fori_loop(1, n_ep, greet, 0)
-
     firsts = [
         pltpu.make_async_copy(src, dst, isem.at[i])
         for i, (src, dst) in enumerate(
@@ -172,11 +157,23 @@
             ]
         )
     ]
+    barrier = pltpu.get_barrier_semaphore()
+    for peer in (x_plus, x_minus, y_plus, y_minus):
+        pl.semaphore_signal(barrier, inc=1, device_id=peer, device_id_type=MESH)
+
+    def greet(o, carry):
+        pl.semaphore_signal(
+            barrier, inc=1, device_id=(lax.rem(ep + o, n_ep), tp), device_id_type=MESH
+        )
+        return carry
+
+    lax.fori_loop(1, n_ep, greet, 0)
+
+    for first in firsts:
+        first.wait()
     for load in loads:
         load.start()
 
-    for first in firsts:
-        first.wait()
 
     gains[0 : SIDE * SIDE] = mix_gain[...].astype(F32).reshape(SIDE * SIDE, 1, COL)
     gains[SIDE * SIDE :] = moe_gain[...].astype(F32).reshape(SIDE * SIDE, 1, COL)
@@ -216,7 +213,7 @@
     half_ep = n_ep // 2
 
     def dispatch_copy(i):
-        u, c = i // 2, lax.rem(i, 2)
+        u, c = i // 2, i % 2
         peer = partner(u, c, False)
         return pltpu.make_async_remote_copy(
             src_ref=slots.at[peer],
@@ -228,7 +225,7 @@
         )
 
     def return_copy(i, chunk):
-        u, c = i // 2, lax.rem(i, 2)
+        u, c = i // 2, i % 2
         peer = partner(u, c, True)
         return pltpu.make_async_remote_copy(
             src_ref=outgoing.at[i],
@@ -241,15 +238,24 @@
 
     own_place = 2 * near_z + core
 
-    def send_all(make, first, count):
-        def send(i, carry):
-            @pl.when(i != own_place)
-            def _():
-                make(i).start()
-
-            return carry
-
-        lax.fori_loop(first, first + count, send, 0)
+    def send_all(make, chunk):
+        half_z = n_z // 2
+        ways = range(half_z * chunk, half_z * (chunk + 1))
+
+        def far(u):
+            ahead = (u - near_z) % n_z
+            return -min(ahead, n_z - ahead)
+
+        for u in sorted(ways, key=far):
+            for c in range(2):
+                copy = make(2 * u + c)
+                if u != near_z:
+                    copy.start()
+                else:
+
+                    @pl.when(core != c)
+                    def _():
+                        copy.start()
 
     def whole(src, dst, k, count, r=None):
         return pltpu.make_async_remote_copy(
@@ -337,14 +343,20 @@
         for g in pair:
             g.cross(0, 4)
 
-    def gather_near(pair):
+    def gather_near_a(pair):
         for g in pair:
             g.near()
         for g in pair:
             g.cross(-1, 8)
             g.cross(1, 12)
+
+    def gather_near_b(pair):
         for g in pair:
             g.relay(0, 4)
+
+    def gather_near(pair):
+        gather_near_a(pair)
+        gather_near_b(pair)
 
     def gather_far(pair):
         for g in pair:
@@ -584,10 +596,6 @@
         return got
 
     live = {}
-    stores = [
-        pltpu.make_async_copy(mix_out, mix_out_h, osem.at[0]),
-        pltpu.make_async_copy(moe_out, moe_out_h, osem.at[1]),
-    ]
     mix = gathers(xa, xb, agx_s, agx_r)
     xo = [(wm, acc_x)]
 
@@ -596,6 +604,12 @@
 
     def x_near():
         gather_near(mix)
+
+    def x_near_a():
+        gather_near_a(mix)
+
+    def x_near_b():
+        gather_near_b(mix)
 
     def x_far():
         gather_far(mix)
@@ -798,7 +812,7 @@
             got = jnp.concatenate(scatter_end(self.sums), axis=0)
             first = half_ep * self.c
             outgoing[first : first + half_ep] = got.reshape(half_ep, cap, COL).astype(BF16)
-            send_all(lambda i: return_copy(i, self.c), first, half_ep)
+            send_all(lambda i: return_copy(i, self.c), self.c)
             if self.c == 0:
                 returned[ep] = outgoing[own_place]
 
@@ -840,7 +854,6 @@
         got = scatter_end(live["sums"])
         mix_out[0:half_x] = got[0].astype(BF16)
         mix_out[half_x : 2 * half_x] = got[1].astype(BF16)
-        stores[0].start()
 
     def weigh():
         score0, score1 = places[:, 2:3], places[:, 3:4]
@@ -857,13 +870,14 @@
         whole(outgoing, returned, 1, half_ep, 3).wait_recv()
         results = returned[...].astype(F32).reshape(n_ep * cap, COL).astype(BF16)
         moe_out[...] = (dot(live["coarse"], results) + dot(live["fine"], results)).astype(BF16)
-        stores[1].start()
-
-    send_all(dispatch_copy, 0, half_ep)
+
+    send_all(dispatch_copy, 0)
     x_start()
     arrived[own_place] = slots[ep]
-    x_near()
-    send_all(dispatch_copy, half_ep, half_ep)
+    weigh()
+    x_near_a()
+    send_all(dispatch_copy, 1)
+    x_near_b()
     near_chunk.start()
     x_far()
     near_chunk.near()
@@ -872,8 +886,8 @@
     far_chunk.start()
     x_last()
     near_chunk.relays()
+    recurrence()
     far_chunk.near()
-    recurrence()
     near_chunk.last()
     far_chunk.far()
     near_chunk.experts()
@@ -881,11 +895,11 @@
     far_chunk.relays()
     near_chunk.sum_direct()
     near_chunk.sum_own()
+    chain_states()
     far_chunk.last()
     far_chunk.experts()
     far_chunk.sum_start()
     far_chunk.sum_direct()
-    chain_states()
     far_chunk.sum_relay(0)
     far_chunk.sum_relay(1)
     far_chunk.sum_own()
@@ -906,7 +920,6 @@
     x_sum_settle(0)
     x_sum_settle(1)
     x_sum_relay2()
-    weigh()
     x_store()
     combine()
 
@@ -921,9 +934,6 @@
     @pl.when(not_owner)
     def _():
         whole(st_out, st_in, 2, slices).wait_send()
-
-    for store in stores:
-        store.wait()
 
 
 def per_device(n_ep, *args):
@@ -983,8 +993,6 @@
         v((1, COL)),
         v((2, tok_b), jnp.int32),
         v((2, tok_b), F32),
-        v((tok_a, COL)),
-        v((tok_b, COL)),
         v((width, 4 * COL)),
         v((COL, width)),
         v((hidden, width)),
@@ -1014,7 +1022,6 @@
         *scatter_ends(hx),
         *scatter_ends(hm, (2,)),
         dma((9,)),
-        dma((2,)),
         dma((8,)),
         dma((4,)),
         dma((6,)),
@@ -1030,14 +1037,14 @@
     return pl.pallas_call(
         functools.partial(step_kernel, n_ep, cap),
         out_shape=[
-            jax.ShapeDtypeStruct((tok_a, COL), BF16),
-            jax.ShapeDtypeStruct((tok_b, COL), BF16),
+            v((tok_a, COL)),
+            v((tok_b, COL)),
         ],
         in_specs=[hbm] * 17,
-        out_specs=[hbm, hbm],
+        out_specs=[pl.BlockSpec(memory_space=pltpu.VMEM)] * 2,
         scratch_shapes=scratch,
         compiler_params=pltpu.CompilerParams(
-            collective_id=0, has_side_effects=True, vmem_limit_bytes=63 * 1024 * 1024
+            collective_id=0, has_side_effects=True, vmem_limit_bytes=62 * 1024 * 1024
         ),
     )(
         mix_rows,

time: 81.9 us -> 80.3 us (0.980); the launches traced: 81.7 us -> 78.8 us
  Pallas kernels: 78.9 us -> 76.9 us
  local copies, waits for them, and re-layouts: 2.14 us -> 1.26 us
    pallas_call x1, Pallas kernels: 78.9 us -> 76.9 us  [per_device(): pl.pallas_call(functools.partial(step_kernel, n_ep, cap), out_shape=[v((t...]
    unnamed x4 -> x2, local copies, waits for them, and re-layouts: 2.14 us -> 1.26 us
where the time goes in v4:
time: 80.3 us; the launch traced here: 78.8 us
  Pallas kernels  76.9 us (96%)
  local copies, waits for them, and re-layouts  1.26 us (2%)
    pallas_call x1, Pallas kernels, per_device(): pl.pallas_call(functools.partial(step_kernel, n_ep, cap), out_shape=[v((t...  76.9 us

profile of v4, /device:TPU:1, one launch (start us, length us, event | category | flops | bytes accessed | tf_op | source)
XLA Modules:
  0.0 78.8 jit_solution(18075743073881617799)
XLA Ops:
  0.6 76.9 %shard_map.176 = (bf16[256,128]{1,0:T(8,128)(2,1)S(1)}, bf16[256,128]{1,0:T(8,128)(2,1)S(1)}) custom-call(bf16[256,128]{1,0:T(8,128)(2,1)} %mix_rows_h.1, bf16[256,128]{1,0:T(8,128)(2,1)} %moe_rows_h.1, bf16[16,128]{1,0:T(8,128)(2,1)} %bitcast.10, bf16[16,128]{1,0:T(8,128)(2,1)} %bitcast.11, f32[1,128]{1,0:T(1,128)} %bitcast.14, f32[1,256]{1,0:T(1,128)} %decay_h.1, ...), custom_call_target="tpu_custom_call" | custom-call | tf_op jit(solution)/shard_map/pallas_call | solution.py:1037
  77.5 0.6 copy.21
  78.1 0.6 copy.22
